TPU v7x, 32 devices: a whole 2x2x4 slice. The times are simulated.
32 devices in a mesh: ep: 16 (over z, y, x), tp: 2 (over core).
Axes of the slice: x: 2, y: 2, z: 4, core: 2. Of those that a mesh axis runs over, the one named last changes fastest.
Arguments:
- tokens: bfloat16 [32, 2048], P('ep'), may hold values from -6 to 6
- head_state: float32 [32, 32, 64, 128], P('ep', 'tp'), may hold values from -4 to 4
- conv_state: bfloat16 [32, 3, 2048], P('ep', None, 'tp'), may hold values from -6 to 6
- conv_proj_state: bfloat16 [32, 3, 2, 512], P('ep', None, None, 'tp'), may hold values from -6 to 6
- first_gain: float32 [2048], replicated, may hold values from 0.1 to 1.9
- gate_weight: bfloat16 [2048, 2048], P('ep', 'tp'), may hold values from -0.125 to 0.125
- inner_weight: bfloat16 [2048, 2048], P('ep', 'tp'), may hold values from -0.125 to 0.125
- write_weight: bfloat16 [2048, 512], P(None, 'tp'), may hold values from -0.125 to 0.125
- read_weight: bfloat16 [2048, 512], P(None, 'tp'), may hold values from -0.125 to 0.125
- step_weight: bfloat16 [2048, 32], P(None, 'tp'), may hold values from -0.125 to 0.125
- conv_kernel: float32 [4, 2048], P(None, 'tp'), may hold values from -3 to 3
- conv_proj_kernel: float32 [4, 2, 512], P(None, None, 'tp'), may hold values from -3 to 3
- step_bias: float32 [32], P('tp'), may hold values from -2 to 1
- log_rate: float32 [32], P('tp'), may hold values from -4.5 to 1.5
- skip_gain: float32 [32], P('tp'), may hold values from 0.5 to 2
- group_gain: float32 [2048], P('tp'), may hold values from 0.1 to 1.9
- out_weight: bfloat16 [2048, 2048], P('tp', 'ep'), may hold values from -0.125 to 0.125
- second_gain: float32 [2048], replicated, may hold values from 0.1 to 1.9
- routes: int32 [32, 4], P('ep'), may hold values from 0 to 15, all different within a row; in each aligned block of 32 rows (0 to 31, 32 to 63, ...) at most 32 rows name the same one
- route_logits: bfloat16 [32, 4], P('ep'), may hold values from -8 to 300
- expert_gate: bfloat16 [16, 2048, 1024], P('ep', None, 'tp'), may hold values from -0.5 to 0.5
- expert_up: bfloat16 [16, 2048, 1024], P('ep', None, 'tp'), may hold values from -0.5 to 0.5
- expert_down: bfloat16 [16, 1024, 2048], P('ep', 'tp'), may hold values from -0.0234375 to 0.0234375
- dense_up: bfloat16 [2048, 4096], P(None, ('ep', 'tp')), may hold values from -0.125 to 0.125
- dense_down: bfloat16 [4096, 2048], P(('ep', 'tp')), may hold values from -0.09375 to 0.09375
- dense_gate: float32 [2048], replicated, may hold values from -0.125 to 0.125
Outputs:
- layer_out: bfloat16 [32, 2048], P(('ep', 'tp'))
- state_out: float32 [32, 32, 64, 128], P('ep', 'tp')
- conv_out: bfloat16 [32, 3, 2048], P('ep', None, 'tp')
- conv_proj_out: bfloat16 [32, 3, 2, 512], P('ep', None, None, 'tp')
Inputs may be any that keep to these rules, and one draw needn't show every extreme that they name: `routes`: each token names 4 different experts; over the whole batch no expert is named by more than 32 rows, a bound that some block reaches.
All inputs are finite; a program needn't handle non-finite values.
Results may differ from a plain program's by a relative error of at most 0.015.
Values may be sent and summed in bfloat16 or wider, within the bound.
No kernel may reach another device: no remote copies, remote signals or barrier semaphores. Data moves between devices by JAX's collectives and lax.ppermute only.
A program may use at most 64 MiB of HBM per device.

v0:
```python
import jax
import jax.numpy as jnp
from jax import lax
from jax.sharding import PartitionSpec as P

GROUPS = 4


norm_eps = 1e-05
clamp_limit = 7.0
glu_alpha = 1.702
highest = lax.Precision.HIGHEST


def rms_scale(values, gain_vec):
    return (
        values * lax.rsqrt(jnp.mean(values * values, axis=-1, keepdims=True) + norm_eps) * gain_vec
    )


def clamped_unit(gate_pre, up_pre):
    glu_part = jnp.minimum(gate_pre, clamp_limit)
    lin_part = jnp.clip(up_pre, -clamp_limit, clamp_limit)
    return glu_part * jax.nn.sigmoid(glu_alpha * glu_part) * (lin_part + 1.0)


def state_step(
    inner_proj,
    gate_proj,
    write_proj,
    read_proj,
    step_raw,
    conv_state,
    conv_proj_state,
    conv_kernel,
    conv_proj_kernel,
    step_bias,
    log_rate,
    skip_gain,
    group_gain,
    head_state,
    group_count,
):
    window_inner = jnp.concatenate([conv_state, inner_proj[:, None, :]], axis=1)
    window_proj = jnp.concatenate(
        [conv_proj_state, jnp.stack([write_proj, read_proj], axis=1)[:, None]], axis=1
    )
    conv_inner = jax.nn.silu(jnp.sum(window_inner.astype(jnp.float32) * conv_kernel[None], axis=1))
    conv_proj = jax.nn.silu(
        jnp.sum(window_proj.astype(jnp.float32) * conv_proj_kernel[None], axis=1)
    )
    seq_count, channels = conv_inner.shape
    head_count = step_raw.shape[1]
    head_width = channels // head_count
    state_width = conv_proj.shape[2] // group_count
    per_group = head_count // group_count
    head_input = conv_inner.reshape(seq_count, head_count, head_width)
    write_heads = jnp.repeat(
        conv_proj[:, 0].reshape(seq_count, group_count, state_width), per_group, axis=1
    )
    read_heads = jnp.repeat(
        conv_proj[:, 1].reshape(seq_count, group_count, state_width), per_group, axis=1
    )
    step_size = jax.nn.softplus(step_raw + step_bias)
    decay_rate = jnp.exp(-jnp.exp(log_rate) * step_size)
    state_out = (
        decay_rate[:, :, None, None] * head_state
        + (step_size[:, :, None] * head_input)[:, :, :, None] * write_heads[:, :, None, :]
    )
    read_out = (
        jnp.einsum("shpn,shn->shp", state_out, read_heads, precision=highest)
        + skip_gain[None, :, None] * head_input
    )
    gated_rows = read_out.reshape(seq_count, channels) * jax.nn.silu(gate_proj.astype(jnp.float32))
    grouped = gated_rows.reshape(seq_count, group_count, channels // group_count)
    grouped = grouped * lax.rsqrt(jnp.mean(grouped * grouped, axis=-1, keepdims=True) + norm_eps)
    mixer_rows = (grouped.reshape(seq_count, channels) * group_gain).astype(jnp.bfloat16)
    return (mixer_rows, state_out, window_inner[:, 1:], window_proj[:, 1:])


def local(
    tokens,
    head_state,
    conv_state,
    conv_proj_state,
    first_gain,
    gate_weight,
    inner_weight,
    write_weight,
    read_weight,
    step_weight,
    conv_kernel,
    conv_proj_kernel,
    step_bias,
    log_rate,
    skip_gain,
    group_gain,
    out_weight,
    second_gain,
    routes,
    route_logits,
    expert_gate,
    expert_up,
    expert_down,
    dense_up,
    dense_down,
    dense_gate,
):
    seq_count = tokens.shape[0]
    half_width = gate_weight.shape[1]
    normed_in = rms_scale(tokens.astype(jnp.float32), first_gain).astype(jnp.bfloat16)
    features = lax.all_to_all(normed_in, "ep", split_axis=1, concat_axis=0, tiled=True)
    row_block = features
    both_terms = lax.psum_scatter(
        jnp.concatenate(
            [
                jnp.dot(row_block, gate_weight, preferred_element_type=jnp.float32),
                jnp.dot(row_block, inner_weight, preferred_element_type=jnp.float32),
            ],
            axis=1,
        ),
        "ep",
        scatter_dimension=0,
        tiled=True,
    )
    gate_sum = both_terms[:, :half_width]
    inner_sum = both_terms[:, half_width:]
    gate_proj = gate_sum.astype(jnp.bfloat16)
    inner_proj = inner_sum.astype(jnp.bfloat16)
    write_proj = jnp.dot(normed_in, write_weight, preferred_element_type=jnp.float32).astype(
        jnp.bfloat16
    )
    read_proj = jnp.dot(normed_in, read_weight, preferred_element_type=jnp.float32).astype(
        jnp.bfloat16
    )
    step_raw = jnp.dot(normed_in, step_weight, preferred_element_type=jnp.float32)
    local_groups = GROUPS // lax.axis_size("tp")
    mixer_rows, state_out, conv_out, conv_proj_out = state_step(
        inner_proj,
        gate_proj,
        write_proj,
        read_proj,
        step_raw,
        conv_state,
        conv_proj_state,
        conv_kernel,
        conv_proj_kernel,
        step_bias,
        log_rate,
        skip_gain,
        group_gain,
        head_state,
        local_groups,
    )
    partial_mix = jnp.dot(
        mixer_rows,
        lax.all_gather(out_weight, "ep", axis=1, tiled=True),
        preferred_element_type=jnp.float32,
    )
    mixed = lax.psum(partial_mix, "tp")
    hidden = (tokens.astype(jnp.float32) + mixed).astype(jnp.bfloat16)
    normed_mid = rms_scale(hidden.astype(jnp.float32), second_gain).astype(jnp.bfloat16)
    all_rows, all_routes, all_logits = (
        lax.all_gather(normed_mid, "ep", axis=0, tiled=True),
        lax.all_gather(routes, "ep", axis=0, tiled=True),
        lax.all_gather(route_logits, "ep", axis=0, tiled=True),
    )
    route_gates = jax.nn.softmax(all_logits.astype(jnp.float32), axis=-1)
    my_expert = lax.axis_index("ep")
    route_hits = all_routes == my_expert
    row_weight = jnp.sum(jnp.where(route_hits, route_gates, 0.0), axis=1)
    chosen = jnp.any(route_hits, axis=1)
    slot_index = jnp.cumsum(chosen.astype(jnp.int32)) - 1
    capacity = 4 * seq_count * routes.shape[1]
    slot_ids = jnp.arange(capacity, dtype=jnp.int32)
    picks = (slot_index[None, :] == slot_ids[:, None]) & chosen[None, :]
    picked_rows = jnp.dot(
        picks.astype(jnp.bfloat16), all_rows, preferred_element_type=jnp.float32
    ).astype(jnp.bfloat16)
    activated = clamped_unit(
        jnp.dot(picked_rows, expert_gate[0], preferred_element_type=jnp.float32),
        jnp.dot(picked_rows, expert_up[0], preferred_element_type=jnp.float32),
    ).astype(jnp.bfloat16)
    expert_part = jnp.dot(activated, expert_down[0], preferred_element_type=jnp.float32)
    placed = jnp.where(picks, row_weight[None, :], 0.0)
    dense_weight = jax.nn.sigmoid(
        jnp.dot(all_rows.astype(jnp.float32), dense_gate, precision=highest)
    )
    row_share = seq_count // lax.axis_size("tp")
    row_block = all_rows
    dense_inner = jax.nn.silu(
        jnp.dot(row_block, dense_up, preferred_element_type=jnp.float32)
    ).astype(jnp.bfloat16)
    dense_term = (
        jnp.dot(dense_inner, dense_down, preferred_element_type=jnp.float32) * dense_weight[:, None]
    )
    summed = lax.psum_scatter(
        dense_term + jnp.einsum("cr,cd->rd", placed, expert_part, precision=highest),
        ("ep", "tp"),
        scatter_dimension=0,
        tiled=True,
    )
    own_rows = lax.dynamic_slice_in_dim(hidden, lax.axis_index("tp") * row_share, row_share, 0)
    layer_out = (own_rows.astype(jnp.float32) + summed).astype(jnp.bfloat16)
    return (layer_out, state_out, conv_out, conv_proj_out)


def solution(mesh):
    placed = (
        P("ep", None),
        P("ep", "tp", None, None),
        P("ep", None, "tp"),
        P("ep", None, None, "tp"),
        P(),
        P("ep", "tp"),
        P("ep", "tp"),
        P(None, "tp"),
        P(None, "tp"),
        P(None, "tp"),
        P(None, "tp"),
        P(None, None, "tp"),
        P("tp"),
        P("tp"),
        P("tp"),
        P("tp"),
        P("tp", "ep"),
        P(),
        P("ep", None),
        P("ep", None),
        P("ep", None, "tp"),
        P("ep", None, "tp"),
        P("ep", "tp", None),
        P(None, ("ep", "tp")),
        P(("ep", "tp"), None),
        P(),
    )
    return jax.shard_map(
        local,
        mesh=mesh,
        in_specs=placed,
        out_specs=(
            P(("ep", "tp"), None),
            P("ep", "tp", None, None),
            P("ep", None, "tp"),
            P("ep", None, None, "tp"),
        ),
        check_vma=False,
    )
```

profile of v0, /device:TPU:0, one launch (start us, length us, event | category | flops | bytes accessed | tf_op | source)
XLA Modules:
  0.0 366.6 jit_solution(6671447801654428181)
XLA Ops:
  7.3 0.7 all-gather.5.cloned.1.call-update
  8.0 0.9 fusion.43
  8.9 1.4 fusion.107
  10.3 8.3 %all-to-all-start = ((bf16[2,16,128]{2,0,1:T(2,128)(2,1)}), bf16[2,16,128]{2,0,1:T(2,128)(2,1)S(1)}, u32[]{:S(2)}, u32[]{:S(2)}) async-start(bf16[2,16,128]{2,0,1:T(2,128)(2,1)} %fusion.107), calls=%async_computation | async-start | bytes 16384 | tf_op jit(solution)/shard_map/all_to_all | solution.py:112
  18.7 41.6 %all-gather.1 = s32[16,2,4]{2,1,0:T(2,128)S(1)} all-gather(s32[1,2,4]{2,1,0:T(2,128)} %bitcast.98), channel_id=1, replica_groups=mesh['ep'=16,'tp'=2] {'ep'}, dimensions={0}, use_global_device_ids=true | all-gather | bytes 544 | tf_op jit(solution)/shard_map/all_gather | solution.py:165
  60.4 0.4 fusion.77
  60.9 36.8 %all-gather.2 = bf16[16,2,4]{2,1,0:T(2,128)(2,1)S(1)} all-gather(bf16[1,2,4]{2,1,0:T(2,128)(2,1)} %bitcast.99), channel_id=1, replica_groups=mesh['ep'=16,'tp'=2] {'ep'}, dimensions={0}, use_global_device_ids=true | all-gather | bytes 272 | tf_op jit(solution)/shard_map/all_gather | solution.py:166
  97.8 0.1 reshape.123
  98.2 1.5 fusion.24
  99.7 1.5 fusion.25
  101.3 0.1 add_reduce_fusion
  101.6 0.2 multiply_exponential_fusion
  101.8 0.6 dynamic-slice
  103.1 0.2 fusion.82
  103.3 0.2 fusion.83
  103.5 75.9 %all-reduce.6 = bf16[32,2048]{1,0:T(8,128)(2,1)S(1)} all-reduce(f32[32,2048]{1,0:T(8,128)S(1)} %pad_maximum_fusion), channel_id=2, replica_groups=mesh['ep'=16,'tp'=2] {'ep'}, use_global_device_ids=true, to_apply=%region_1.0.clone | all-reduce | flops 65536 | bytes 393216
  179.6 1.6 multiply_add_fusion
  181.2 1.7 fusion.84
  183.4 2.8 fusion.65
  186.3 3.4 psum.7
  189.6 0.1 fusion.40
  189.9 36.5 %all-gather = bf16[16,2,2048]{2,1,0:T(2,128)(2,1)S(1)} all-gather(bf16[1,2,2048]{2,1,0:T(2,128)(2,1)S(1)} %fusion.62), channel_id=1, replica_groups=mesh['ep'=16,'tp'=2] {'ep'}, dimensions={0}, use_global_device_ids=true | all-gather | bytes 139264 | tf_op jit(solution)/shard_map/all_gather | solution.py:164
  226.4 0.2 convolution_convert_fusion
  226.6 0.2 fusion.29
  226.7 2.1 fusion.7
  228.9 2.5 fusion.1
  231.4 0.4 fusion.47
  231.9 2.2 fusion
  234.1 0.6 slice.32
  234.7 0.6 fusion.52
  235.3 123.0 %all-reduce.5.cloned.1.call-done = f32[32,2048]{1,0:T(8,128)} async-done(((f32[32,2048]{1,0:T(8,128)}), f32[32,2048]{1,0:T(8,128)}) %all-reduce.5.cloned.1.call-update) | async-done | bytes 262160
  358.3 1.5 fusion.56
  (80 shorter events, 1.7 us)
Async XLA Ops:
  7.2 221.7 %copy-start = (bf16[1,512,2048]{2,1,0:T(8,128)(2,1)S(1)}, bf16[1,512,2048]{2,1,0:T(8,128)(2,1)}, u32[]{:S(2)}) copy-start(bf16[1,512,2048]{2,1,0:T(8,128)(2,1)} %param.48) | copy-start | bytes 6291460
  7.2 94.7 %copy-start.18 = (u32[32]{0:T(128)S(1)}, u32[32]{0:T(128)}, u32[]{:S(2)}) copy-start(u32[32]{0:T(128)} %constant.66) | copy-start | bytes 388
  7.2 94.4 %copy-start.5 = (bf16[2,2048]{1,0:T(2,128)(2,1)S(1)}, bf16[2,2048]{1,0:T(2,128)(2,1)}, u32[]{:S(2)}) copy-start(bf16[2,2048]{1,0:T(2,128)(2,1)} %param.26) | copy-start | bytes 24580
  7.2 94.4 %copy-start.6 = (f32[2048]{0:T(1024)S(1)}, f32[2048]{0:T(1024)}, u32[]{:S(2)}) copy-start(f32[2048]{0:T(1024)} %param.30) | copy-start | bytes 24580
  7.2 94.1 %copy-start.11 = (bf16[2,3,2,256]{3,2,1,0:T(2,128)(2,1)S(1)}, bf16[2,3,2,256]{3,2,1,0:T(2,128)(2,1)}, u32[]{:S(2)}) copy-start(bf16[2,3,2,256]{3,2,1,0:T(2,128)(2,1)} %param.29) | copy-start | bytes 18436
  7.2 94.2 %copy-start.10 = (f32[4,2,256]{2,1,0:T(2,128)S(1)}, f32[4,2,256]{2,1,0:T(2,128)}, u32[]{:S(2)}) copy-start(f32[4,2,256]{2,1,0:T(2,128)} %param.37) | copy-start | bytes 24580
  7.2 94.2 %copy-start.16 = (f32[16]{0:T(128)S(1)}, f32[16]{0:T(128)}, u32[]{:S(2)}) copy-start(f32[16]{0:T(128)} %param.39) | copy-start | bytes 196
  7.2 94.3 %copy-start.14 = (bf16[2048,16]{0,1:T(8,128)(2,1)S(1)}, bf16[2048,16]{0,1:T(8,128)(2,1)}, u32[]{:S(2)}) copy-start(bf16[2048,16]{0,1:T(8,128)(2,1)} %param.35) | copy-start | bytes 196612
  7.3 94.3 %copy-start.17 = (f32[16]{0:T(128)S(1)}, f32[16]{0:T(128)}, u32[]{:S(2)}) copy-start(f32[16]{0:T(128)} %param.38) | copy-start | bytes 196
  7.3 95.8 %copy-start.3 = (bf16[128,1024]{1,0:T(8,128)(2,1)S(1)}, bf16[128,1024]{1,0:T(8,128)(2,1)}, u32[]{:S(2)}) copy-start(bf16[128,1024]{1,0:T(8,128)(2,1)} %param.31) | copy-start | bytes 786436
  7.3 96.0 %copy-start.4 = (bf16[128,1024]{1,0:T(8,128)(2,1)S(1)}, bf16[128,1024]{1,0:T(8,128)(2,1)}, u32[]{:S(2)}) copy-start(bf16[128,1024]{1,0:T(8,128)(2,1)} %param.32) | copy-start | bytes 786436
  7.3 176.1 %all-gather.5.cloned.1.call-start = ((), (), s32[]{:S(2)}) async-start(), calls=%async_computation.1 | async-start | bytes 4456448 | tf_op jit(solution)/shard_map/all_gather | solution.py:157
  10.3 92.8 %all-to-all-start = ((bf16[2,16,128]{2,0,1:T(2,128)(2,1)}), bf16[2,16,128]{2,0,1:T(2,128)(2,1)S(1)}, u32[]{:S(2)}, u32[]{:S(2)}) async-start(bf16[2,16,128]{2,0,1:T(2,128)(2,1)} %fusion.107), calls=%async_computation | async-start | bytes 16384 | tf_op jit(solution)/shard_map/all_to_all | solution.py:112
  18.7 339.6 %all-reduce.5.cloned.1.call-start = ((), (), s32[]{:S(2)}) async-start(), calls=%async_computation.2 | async-start | bytes 524288
  98.0 81.4 %copy-start.7 = (bf16[2,3,1024]{2,0,1:T(2,128)(2,1)S(1)}, bf16[2,3,1024]{2,0,1:T(2,128)(2,1)}, u32[]{:S(2)}) copy-start(bf16[2,3,1024]{2,0,1:T(2,128)(2,1)} %param.28) | copy-start | bytes 36868
  98.0 81.4 %copy-start.8 = (f32[4,1024]{1,0:T(4,128)S(1)}, f32[4,1024]{1,0:T(4,128)}, u32[]{:S(2)}) copy-start(f32[4,1024]{1,0:T(4,128)} %param.36) | copy-start | bytes 49156
  103.4 79.5 %copy-start.13 = (f32[16]{0:T(128)S(1)}, f32[16]{0:T(128)}, u32[]{:S(2)}) copy-start(f32[16]{0:T(128)} %param.40) | copy-start | bytes 196
  103.4 80.0 %copy-start.12 = (f32[1024]{0:T(1024)S(1)}, f32[1024]{0:T(1024)}, u32[]{:S(2)}) copy-start(f32[1024]{0:T(1024)} %param.41) | copy-start | bytes 12292
  181.2 5.1 %copy-start.1 = (f32[2,16,64,128]{3,2,1,0:T(8,128)}, f32[2,16,64,128]{3,2,1,0:T(8,128)S(1)}, u32[]{:S(2)}) copy-start(f32[2,16,64,128]{3,2,1,0:T(8,128)S(1)} %multiply_add_fusion) | copy-start | bytes 3145732
  183.4 6.4 %copy-start.9 = (f32[2048]{0:T(1024)S(1)}, f32[2048]{0:T(1024)}, u32[]{:S(2)}) copy-start(f32[2048]{0:T(1024)} %param.43) | copy-start | bytes 24580
  183.4 43.1 %copy-start.15 = (f32[2048]{0:T(1024)S(1)}, f32[2048]{0:T(1024)}, u32[]{:S(2)}) copy-start(f32[2048]{0:T(1024)} %param.51) | copy-start | bytes 24580
  228.9 3.0 copy-start.2
Sparse Core Ops, SparseCore 0:
  10.8 92.4 all-gather.4
  234.2 124.0 all-reduce.4
where the time goes:
time: 367 us
  blocking collectives  194 us (53%)
  waiting for transfers between devices  124 us (34%)
  matrix products  15.7 us (4%)
  between operations  15.2 us (4%)
  starting transfers between devices  8.42 us (2%)
  other arithmetic  7.27 us (2%)
    unnamed x3, waiting for transfers between devices  124 us
    unnamed x1, blocking collectives  75.9 us
    all_gather x1, blocking collectives, local(): lax.all_gather(routes, 'ep', axis=0, tiled=True)  41.6 us
    all_gather x1, blocking collectives, local(): lax.all_gather(route_logits, 'ep', axis=0, tiled=True)  36.8 us
    all_gather x1, blocking collectives, local(): lax.all_gather(normed_mid, 'ep', axis=0, tiled=True)  36.5 us
    all_to_all x1, starting transfers between devices, local(): lax.all_to_all(normed_in, 'ep', split_axis=1, concat_axis=0, tiled=True)  8.34 us
  transfers between devices with their start and end apart: 3, of which 1 were waited for; matrix products, arithmetic and copies ran while one was open for 4% of the time, Pallas kernels for 0%

commit v1 on v0

v1 whole, which is shorter than its diff:
```python
import jax
import jax.numpy as jnp
from jax import lax
from jax.sharding import PartitionSpec as P

GROUPS = 4
TAIL = 128

norm_eps = 1e-05
clamp_limit = 7.0
glu_alpha = 1.702
highest = lax.Precision.HIGHEST
f32 = jnp.float32
bf16 = jnp.bfloat16


def clamped_unit(gate_pre, up_pre):
    glu_part = jnp.minimum(gate_pre, clamp_limit)
    lin_part = jnp.clip(up_pre, -clamp_limit, clamp_limit)
    return glu_part * jax.nn.sigmoid(glu_alpha * glu_part) * (lin_part + 1.0)


def state_step(
    inner_proj,
    gate_proj,
    write_proj,
    read_proj,
    step_raw,
    conv_state,
    conv_proj_state,
    conv_kernel,
    conv_proj_kernel,
    step_bias,
    log_rate,
    skip_gain,
    group_gain,
    head_state,
    group_count,
):
    window_inner = jnp.concatenate([conv_state, inner_proj[:, None, :]], axis=1)
    window_proj = jnp.concatenate(
        [conv_proj_state, jnp.stack([write_proj, read_proj], axis=1)[:, None]], axis=1
    )
    conv_inner = jax.nn.silu(jnp.sum(window_inner.astype(f32) * conv_kernel[None], axis=1))
    conv_proj = jax.nn.silu(jnp.sum(window_proj.astype(f32) * conv_proj_kernel[None], axis=1))
    seq_count, channels = conv_inner.shape
    head_count = step_raw.shape[1]
    head_width = channels // head_count
    state_width = conv_proj.shape[2] // group_count
    per_group = head_count // group_count
    head_input = conv_inner.reshape(seq_count, head_count, head_width)
    write_heads = jnp.repeat(
        conv_proj[:, 0].reshape(seq_count, group_count, state_width), per_group, axis=1
    )
    read_heads = jnp.repeat(
        conv_proj[:, 1].reshape(seq_count, group_count, state_width), per_group, axis=1
    )
    step_size = jax.nn.softplus(step_raw + step_bias)
    decay_rate = jnp.exp(-jnp.exp(log_rate) * step_size)
    state_out = (
        decay_rate[:, :, None, None] * head_state
        + (step_size[:, :, None] * head_input)[:, :, :, None] * write_heads[:, :, None, :]
    )
    read_out = (
        jnp.sum(state_out * read_heads[:, :, None, :], axis=-1)
        + skip_gain[None, :, None] * head_input
    )
    gated_rows = read_out.reshape(seq_count, channels) * jax.nn.silu(gate_proj.astype(f32))
    grouped = gated_rows.reshape(seq_count, group_count, channels // group_count)
    grouped = grouped * lax.rsqrt(jnp.mean(grouped * grouped, axis=-1, keepdims=True) + norm_eps)
    mixer_rows = (grouped.reshape(seq_count, channels) * group_gain).astype(bf16)
    return (mixer_rows, state_out, window_inner[:, 1:], window_proj[:, 1:])


def local(
    tokens,
    head_state,
    conv_state,
    conv_proj_state,
    first_gain,
    gate_weight,
    inner_weight,
    write_weight,
    read_weight,
    step_weight,
    conv_kernel,
    conv_proj_kernel,
    step_bias,
    log_rate,
    skip_gain,
    group_gain,
    out_weight,
    second_gain,
    routes,
    route_logits,
    expert_gate,
    expert_up,
    expert_down,
    dense_up,
    dense_down,
    dense_gate,
):
    n_ep = lax.axis_size("ep")
    n_tp = lax.axis_size("tp")
    n_all = n_ep * n_tp
    my_ep = lax.axis_index("ep")
    my_tp = lax.axis_index("tp")
    seq, width = tokens.shape
    rows = seq * n_ep
    half = gate_weight.shape[1]
    block = gate_weight.shape[0]

    raw_block = lax.all_to_all(tokens, "ep", split_axis=1, concat_axis=0, tiled=True)

    tok = tokens.astype(f32)
    scale = lax.rsqrt(jnp.mean(tok * tok, axis=-1, keepdims=True) + norm_eps)
    normed_in = (tok * scale * first_gain).astype(bf16)
    write_proj = jnp.dot(normed_in, write_weight, preferred_element_type=f32).astype(bf16)
    read_proj = jnp.dot(normed_in, read_weight, preferred_element_type=f32).astype(bf16)
    step_raw = jnp.dot(normed_in, step_weight, preferred_element_type=f32)

    swap = [(i, (i + 1) % n_tp) for i in range(n_tp)]
    other_weight = lax.ppermute(out_weight, "tp", swap)

    gain_block = lax.dynamic_slice_in_dim(first_gain, my_ep * block, block, 0)
    scaled = (raw_block.astype(f32) * gain_block).astype(bf16)
    terms = jnp.concatenate(
        [
            jnp.dot(scaled, gate_weight, preferred_element_type=f32).astype(bf16),
            jnp.dot(scaled, inner_weight, preferred_element_type=f32).astype(bf16),
        ],
        axis=1,
    ).reshape(n_ep, seq, 2 * half)
    terms = lax.all_to_all(terms, "ep", split_axis=0, concat_axis=0, tiled=True)
    both = jnp.sum(terms.astype(f32), axis=0) * scale
    gate_proj = both[:, :half].astype(bf16)
    inner_proj = both[:, half:].astype(bf16)

    mixer_rows, state_out, conv_out, conv_proj_out = state_step(
        inner_proj,
        gate_proj,
        write_proj,
        read_proj,
        step_raw,
        conv_state,
        conv_proj_state,
        conv_kernel,
        conv_proj_kernel,
        step_bias,
        log_rate,
        skip_gain,
        group_gain,
        head_state,
        GROUPS // n_tp,
    )

    top = routes.shape[1]
    tail = jnp.concatenate(
        [routes.astype(bf16), route_logits, jnp.zeros((seq, TAIL - 2 * top), bf16)], axis=1
    )
    packed = jnp.concatenate([mixer_rows, tail], axis=1)
    packed = jnp.broadcast_to(packed[None], (n_all, seq, half + TAIL))
    packed = lax.all_to_all(packed, ("ep", "tp"), split_axis=0, concat_axis=0, tiled=True)
    packed = packed.reshape(n_ep, n_tp, seq, half + TAIL)
    own_half = lax.dynamic_index_in_dim(packed, my_tp, 1, keepdims=False)
    other_half = lax.dynamic_index_in_dim(packed, n_tp - 1 - my_tp, 1, keepdims=False)
    own_half = own_half.reshape(rows, half + TAIL)
    other_half = other_half.reshape(rows, half + TAIL)
    all_routes = own_half[:, half : half + top]
    all_logits = own_half[:, half + top : half + 2 * top]
    mixed = jnp.dot(own_half[:, :half], out_weight, preferred_element_type=f32) + jnp.dot(
        other_half[:, :half], other_weight, preferred_element_type=f32
    )
    hidden_block = (raw_block.astype(f32) + mixed).astype(bf16)

    hidden = jnp.broadcast_to(hidden_block[None], (n_ep, rows, block))
    hidden = lax.all_to_all(hidden, "ep", split_axis=0, concat_axis=0, tiled=True)
    hidden = hidden.transpose(1, 0, 2).reshape(rows, width)

    hid = hidden.astype(f32)
    normed = hid * lax.rsqrt(jnp.mean(hid * hid, axis=-1, keepdims=True) + norm_eps) * second_gain
    normed_mid = normed.astype(bf16)

    route_gates = jax.nn.softmax(all_logits.astype(f32), axis=-1)
    row_weight = jnp.sum(
        jnp.where(all_routes.astype(jnp.int32) == my_ep, route_gates, 0.0), axis=1, keepdims=True
    )
    dense_weight = jax.nn.sigmoid(
        jnp.sum(normed_mid.astype(f32) * dense_gate, axis=-1, keepdims=True)
    )
    activated = clamped_unit(
        jnp.dot(normed_mid, expert_gate[0], preferred_element_type=f32),
        jnp.dot(normed_mid, expert_up[0], preferred_element_type=f32),
    ).astype(bf16)
    dense_inner = jax.nn.silu(
        jnp.dot(normed_mid, dense_up, preferred_element_type=f32)
    ).astype(bf16)
    total = (
        jnp.dot(activated, expert_down[0], preferred_element_type=f32) * row_weight
        + jnp.dot(dense_inner, dense_down, preferred_element_type=f32) * dense_weight
    ).astype(bf16)

    row_share = rows // n_all
    total = total.reshape(n_all, row_share, width)
    total = lax.all_to_all(total, ("ep", "tp"), split_axis=0, concat_axis=0, tiled=True)
    summed = jnp.sum(total.astype(f32), axis=0)
    own_rows = lax.dynamic_slice_in_dim(
        hidden, (my_ep * n_tp + my_tp) * row_share, row_share, 0
    )
    layer_out = (own_rows.astype(f32) + summed).astype(bf16)
    return (layer_out, state_out, conv_out, conv_proj_out)


def solution(mesh):
    placed = (
        P("ep", None),
        P("ep", "tp", None, None),
        P("ep", None, "tp"),
        P("ep", None, None, "tp"),
        P(),
        P("ep", "tp"),
        P("ep", "tp"),
        P(None, "tp"),
        P(None, "tp"),
        P(None, "tp"),
        P(None, "tp"),
        P(None, None, "tp"),
        P("tp"),
        P("tp"),
        P("tp"),
        P("tp"),
        P("tp", "ep"),
        P(),
        P("ep", None),
        P("ep", None),
        P("ep", None, "tp"),
        P("ep", None, "tp"),
        P("ep", "tp", None),
        P(None, ("ep", "tp")),
        P(("ep", "tp"), None),
        P(),
    )
    return jax.shard_map(
        local,
        mesh=mesh,
        in_specs=placed,
        out_specs=(
            P(("ep", "tp"), None),
            P("ep", "tp", None, None),
            P("ep", None, "tp"),
            P("ep", None, None, "tp"),
        ),
        check_vma=False,
    )
```

time: 367 us -> 79.1 us (0.22)
  blocking collectives: 194 us -> 0 us
  waiting for transfers between devices: 124 us -> 32.2 us
  between operations: 15.2 us -> 1.1 us
  starting transfers between devices: 8.42 us -> 21.3 us
    unnamed x3 -> x0, waiting for transfers between devices: 124 us -> none
    all_gather x3 -> x0, blocking collectives: 115 us -> none  [the longest x1 41.6 us: local(): lax.all_gather(routes, 'ep', axis=0, tiled=True)]
    unnamed x1 -> x0, blocking collectives: 75.9 us -> none
    all_to_all x1 -> x5, waiting for transfers between devices: 0.01 us -> 32.2 us  [the longest x1 8.18 us: local(): lax.all_to_all(total, ('ep', 'tp'), split_axis=0, concat_axis=0, tiled=True)]
    all_to_all x1 -> x5, starting transfers between devices: 8.34 us -> 21.1 us  [the longest x1 8.48 us: local(): lax.all_to_all(tokens, 'ep', split_axis=1, concat_axis=0, tiled=True)]
    dot_general x13 -> x10, matrix products: 15.7 us -> 12.9 us  [the longest x1 2.55 us: local(): jnp.dot(activated, expert_down[0], preferred_element_type=f32) * row_weight]
  transfers between devices with their start and end apart: 3 -> 6, of which waited for: 1 -> 5; matrix products, arithmetic and copies ran while one was open for 4% -> 11% of each run, Pallas kernels for 0% -> 0%
where the time goes in v1:
time: 79.1 us; the launch traced here: 78.4 us
  waiting for transfers between devices  32.2 us (41%)
  starting transfers between devices  21.3 us (27%)
  matrix products  12.9 us (16%)
  other arithmetic  5.88 us (7%)
  local copies, waits for them, and re-layouts  5 us (6%)
  between operations  1.1 us (1%)
    all_to_all x1, starting transfers between devices, local(): lax.all_to_all(tokens, 'ep', split_axis=1, concat_axis=0, tiled=True)  8.48 us
    all_to_all x1, waiting for transfers between devices, local(): lax.all_to_all(total, ('ep', 'tp'), split_axis=0, concat_axis=0, tiled=True)  8.18 us
    all_to_all x1, waiting for transfers between devices, local(): lax.all_to_all(hidden, 'ep', split_axis=0, concat_axis=0, tiled=True)  7.53 us
    all_to_all x1, waiting for transfers between devices, local(): lax.all_to_all(packed, ('ep', 'tp'), split_axis=0, concat_axis=0, tiled=T...  7.02 us
    all_to_all x1, waiting for transfers between devices, local(): terms = lax.all_to_all(terms, 'ep', split_axis=0, concat_axis=0, tiled=True)  6.54 us
    all_to_all x1, starting transfers between devices, local(): terms = lax.all_to_all(terms, 'ep', split_axis=0, concat_axis=0, tiled=True)  3.97 us
    all_to_all x1, starting transfers between devices, local(): lax.all_to_all(hidden, 'ep', split_axis=0, concat_axis=0, tiled=True)  3.51 us
    all_to_all x1, waiting for transfers between devices, local(): lax.all_to_all(tokens, 'ep', split_axis=1, concat_axis=0, tiled=True)  2.95 us
  transfers between devices with their start and end apart: 6, of which 5 were waited for; matrix products, arithmetic and copies ran while one was open for 11% of the time, Pallas kernels for 0%

profile of v1, /device:TPU:0, one launch (start us, length us, event | category | flops | bytes accessed | tf_op | source)
XLA Modules:
  0.0 78.4 jit_solution(10981490436863323975)
XLA Ops:
  0.8 8.5 %all-to-all-start = ((bf16[2,16,128]{2,0,1:T(2,128)(2,1)}), bf16[2,16,128]{2,0,1:T(2,128)(2,1)S(1)}, u32[]{:S(2)}, u32[]{:S(2)}) async-start(bf16[2,16,128]{2,0,1:T(2,128)(2,1)} %bitcast.89), calls=%async_computation | async-start | bytes 16384 | tf_op jit(solution)/shard_map/all_to_all | solution.py:113
  9.3 0.9 %fusion.55 = f32[2]{0:T(128)S(1)} fusion(bf16[2,2048]{1,0:T(2,128)(2,1)} %param.26), kind=kLoop, calls=%fused_computation.62 | loop fusion | flops 12286 | bytes 8200 | tf_op jit(solution)/shard_map/reduce_sum | solution.py:116
  10.1 1.6 %fusion.27 = bf16[2,1,256]{2,0,1:T(2,128)(2,1)S(1)} fusion(bf16[2048,256]{1,0:T(8,128)(2,1)} %param.33, bf16[2,2048]{1,0:T(2,128)(2,1)} %param.26, f32[2]{0:T(128)S(1)} %add_rsqrt_fusion.2, f32[2048]{0:T(1024)} %param.30), kind=kOutput, calls=%fused_computation.22 | convolution fusion | flops 2114048 | bytes 1065992 | tf_op jit(solution)/shard_map/dot_general | solution.py:118
  11.8 1.5 %fusion.28 = bf16[2,1,256]{2,0,1:T(2,128)(2,1)S(1)} fusion(bf16[2048,256]{1,0:T(8,128)(2,1)} %param.34, bf16[2,2048]{1,0:T(2,128)(2,1)} %param.26, f32[2]{0:T(128)S(1)} %add_rsqrt_fusion.2, f32[2048]{0:T(1024)} %param.30), kind=kOutput, calls=%fused_computation.23 | convolution fusion | flops 2114048 | bytes 1065992 | tf_op jit(solution)/shard_map/dot_general | solution.py:119
  13.5 2.9 %all-to-all-done = bf16[2,16,128]{2,0,1:T(2,128)(2,1)S(1)} async-done(((bf16[2,16,128]{2,0,1:T(2,128)(2,1)}), bf16[2,16,128]{2,0,1:T(2,128)(2,1)S(1)}, u32[]{:S(2)}, u32[]{:S(2)}) %all-to-all-start) | async-done | bytes 8224 | tf_op jit(solution)/shard_map/all_to_all | solution.py:113
  16.7 1.1 %convolution_convert_fusion = bf16[32,1024]{1,0:T(8,128)(2,1)S(1)} fusion(bf16[128,1024]{1,0:T(8,128)(2,1)} %param.32, f32[32,128]{1,0:T(8,128)S(1)} %bitcast.87, f32[128]{0:T(128)S(1)} %dynamic_slice.13), kind=kOutput, calls=%fused_computation.10 | convolution fusion | flops 8429568 | bytes 344576 | tf_op jit(solution)/shard_map/dot_general | solution.py:130
  17.8 0.8 reshape.146
  18.6 4.0 %all-to-all-start.1 = ((bf16[16,2,2048]{2,1,0:T(2,128)(2,1)}), bf16[16,2,2048]{2,1,0:T(2,128)(2,1)S(1)}, u32[]{:S(2)}, u32[]{:S(2)}) async-start(bf16[16,2,2048]{2,1,0:T(2,128)(2,1)} %reshape.146), calls=%async_computation.1 | async-start | bytes 262144 | tf_op jit(solution)/shard_map/all_to_all | solution.py:134
  22.8 1.1 %multiply_exponential_fusion = (f32[2,16]{1,0:T(2,128)S(1)}, f32[2,16]{1,0:T(2,128)S(1)}) fusion(f32[16]{0:T(128)S(1)} %exponential_negate_fusion, f32[16]{0:T(128)S(1)} %copy-done.17, bf16[2048,16]{0,1:T(8,128)(2,1)} %param.35, bf16[2,2048]{1,0:T(2,128)(2,1)S(1)} %copy-done.4, f32[2]{0:T(128)S(1)} %add_rsqrt_fusion.2, f32[2048]{0:T(1024)S(1)} %copy-done.6), kind=kOutput, calls=%fused_computation.96 | convolution fusion | flops 147712 | bytes 82312 | tf_op jit(solution)/shard_map/dot_general | solution.py:120
  23.8 6.5 %all-to-all-done.1 = bf16[16,2,2048]{2,1,0:T(2,128)(2,1)S(1)} async-done(((bf16[16,2,2048]{2,1,0:T(2,128)(2,1)}), bf16[16,2,2048]{2,1,0:T(2,128)(2,1)S(1)}, u32[]{:S(2)}, u32[]{:S(2)}) %all-to-all-start.1) | async-done | bytes 131104 | tf_op jit(solution)/shard_map/all_to_all | solution.py:134
  30.8 1.4 %multiply_reduce_fusion = (f32[2,16,64]{2,1,0:T(8,128)S(1)}, f32[2,16,64,128]{3,2,1,0:T(8,128)}) fusion(f32[2,16,128]{2,1,0:T(8,128)S(1)} %get-tuple-element.16, f32[2,16,128]{2,1,0:T(8,128)S(1)} %get-tuple-element.17, f32[2,16,64]{2,1,0:T(8,128)S(1)} %multiply_multiply_fusion, f32[2,16,64,128]{3,2,1,0:T(8,128)S(1)} %copy-done.1, ...), kind=kLoop, calls=%fused_computation.25 | loop fusion | flops 1308672 | bytes 2146432 | tf_op jit(solution)/shard_map/reduce_sum | solution.py:65
  32.6 0.7 broadcast_in_dim.22
  33.4 2.6 %all-to-all-start.2 = ((bf16[32,2,1152]{2,1,0:T(2,128)(2,1)}), bf16[32,2,1152]{2,1,0:T(2,128)(2,1)S(1)}, u32[]{:S(2)}, u32[]{:S(2)}) async-start(bf16[32,2,1152]{2,1,0:T(2,128)(2,1)} %broadcast_in_dim.22), calls=%async_computation.2 | async-start | bytes 294912 | tf_op jit(solution)/shard_map/all_to_all | solution.py:163
  36.1 0.6 slice.52
  36.7 0.6 fusion.59
  37.4 7.0 %all-to-all-done.2 = bf16[32,2,1152]{2,1,0:T(2,128)(2,1)S(1)} async-done(((bf16[32,2,1152]{2,1,0:T(2,128)(2,1)}), bf16[32,2,1152]{2,1,0:T(2,128)(2,1)S(1)}, u32[]{:S(2)}, u32[]{:S(2)}) %all-to-all-start.2) | async-done | bytes 147488 | tf_op jit(solution)/shard_map/all_to_all | solution.py:163
  44.6 1.1 %fusion.42 = f32[32,128]{1,0:T(8,128)S(1)} fusion(bf16[1024,128]{1,0:T(8,128)(2,1)} %param.42, bf16[32,1152]{1,0:T(8,128)(2,1)S(1)} %reshape.148), kind=kOutput, calls=%fused_computation.46 | convolution fusion | flops 8388608 | bytes 344064 | tf_op jit(solution)/shard_map/dot_general | solution.py:171
  45.9 0.7 broadcast_in_dim.23
  46.5 3.5 %all-to-all-start.3 = ((bf16[16,32,128]{2,1,0:T(8,128)(2,1)}), bf16[16,32,128]{2,1,0:T(8,128)(2,1)S(1)}, u32[]{:S(2)}, u32[]{:S(2)}) async-start(bf16[16,32,128]{2,1,0:T(8,128)(2,1)} %broadcast_in_dim.23), calls=%async_computation.3 | async-start | bytes 262144 | tf_op jit(solution)/shard_map/all_to_all | solution.py:177
  50.4 0.2 select_reduce_fusion
  50.6 7.5 %all-to-all-done.3 = bf16[16,32,128]{2,1,0:T(8,128)(2,1)S(1)} async-done(((bf16[16,32,128]{2,1,0:T(8,128)(2,1)}), bf16[16,32,128]{2,1,0:T(8,128)(2,1)S(1)}, u32[]{:S(2)}, u32[]{:S(2)}) %all-to-all-start.3) | async-done | bytes 131104 | tf_op jit(solution)/shard_map/all_to_all | solution.py:177
  58.3 0.2 multiply_reduce_fusion.1
  58.5 2.1 %fusion.8 = f32[32,512]{1,0:T(8,128)S(1)} fusion(bf16[1,2048,512]{2,1,0:T(8,128)(2,1)} %param.46, bf16[16,4,8,128]{3,2,1,0:T(8,128)(2,1)S(1)} %get-tuple-element.11), kind=kOutput, calls=%fused_computation.12 | convolution fusion | flops 67125248 | bytes 2293760 | tf_op jit(solution)/shard_map/dot_general | solution.py:192
  60.6 2.5 %convolution_multiply_fusion.1 = f32[32,2048]{1,0:T(8,128)S(1)} fusion(bf16[1,512,2048]{2,1,0:T(8,128)(2,1)S(1)} %copy-done, bf16[1,2048,512]{2,1,0:T(8,128)(2,1)} %param.47, f32[32]{0:T(128)S(1)} %select_reduce_fusion, bf16[16,4,8,128]{3,2,1,0:T(8,128)(2,1)S(1)} %get-tuple-element.11, f32[32,512]{1,0:T(8,128)S(1)} %fusion.8), kind=kOutput, calls=%fused_computation.2 | convolution fusion | flops 134430720 | bytes 4653184 | tf_op jit(solution)/shard_map/dot_general | solution.py:199
  63.2 1.5 %fusion.2 = bf16[32,1,2048]{2,0,1:T(8,128)(2,1)S(1)} fusion(f32[32,2048]{1,0:T(8,128)S(1)} %convolution_multiply_fusion.1, bf16[128,2048]{1,0:T(8,128)(2,1)S(1)} %copy-done.2, f32[32]{0:T(128)S(1)} %add_divide_fusion, bf16[2048,128]{1,0:T(8,128)(2,1)} %param.49, f32[2048]{0:T(1024)S(1)} %copy-done.7, f32[32]{0:T(128)S(1)} %add_rsqrt_fusion.1, ...), kind=kOutput, calls=%fused_computation.4 | convolution fusion | flops 34033664 | bytes 1581312 | tf_op jit(solution)/shard_map/dot_general | solution.py:200
  64.7 0.5 broadcast.136
  65.2 0.7 reduce.4
  65.9 0.7 reshape.153
  66.6 2.6 %all-to-all-start.4 = ((bf16[32,2,1024]{2,1,0:T(2,128)(2,1)}), bf16[32,2,1024]{2,1,0:T(2,128)(2,1)S(1)}, u32[]{:S(2)}, u32[]{:S(2)}) async-start(bf16[32,2,1024]{2,1,0:T(2,128)(2,1)} %reshape.153), calls=%async_computation.4 | async-start | bytes 262144 | tf_op jit(solution)/shard_map/all_to_all | solution.py:205
  69.2 8.2 %all-to-all-done.4 = bf16[32,2,1024]{2,1,0:T(2,128)(2,1)S(1)} async-done(((bf16[32,2,1024]{2,1,0:T(2,128)(2,1)}), bf16[32,2,1024]{2,1,0:T(2,128)(2,1)S(1)}, u32[]{:S(2)}, u32[]{:S(2)}) %all-to-all-start.4) | async-done | bytes 131104 | tf_op jit(solution)/shard_map/all_to_all | solution.py:205
  77.5 0.2 convert_reduce_fusion
  77.7 0.6 add_convert_fusion
  (82 shorter events, 2.6 us)
Async XLA Ops:
  0.6 60.0 %copy-start = (bf16[1,512,2048]{2,1,0:T(8,128)(2,1)S(1)}, bf16[1,512,2048]{2,1,0:T(8,128)(2,1)}, u32[]{:S(2)}) copy-start(bf16[1,512,2048]{2,1,0:T(8,128)(2,1)} %param.48) | copy-start | bytes 6291460
  0.7 22.1 %copy-start.4 = (bf16[2,2048]{1,0:T(2,128)(2,1)S(1)}, bf16[2,2048]{1,0:T(2,128)(2,1)}, u32[]{:S(2)}) copy-start(bf16[2,2048]{1,0:T(2,128)(2,1)} %param.26) | copy-start | bytes 24580
  0.7 12.8 %copy-start.6 = (f32[2048]{0:T(1024)S(1)}, f32[2048]{0:T(1024)}, u32[]{:S(2)}) copy-start(f32[2048]{0:T(1024)} %param.30) | copy-start | bytes 24580
  0.7 12.6 %copy-start.11 = (bf16[2,3,2,256]{3,2,1,0:T(2,128)(2,1)S(1)}, bf16[2,3,2,256]{3,2,1,0:T(2,128)(2,1)}, u32[]{:S(2)}) copy-start(bf16[2,3,2,256]{3,2,1,0:T(2,128)(2,1)} %param.29) | copy-start | bytes 18436
  0.7 12.7 %copy-start.10 = (f32[4,2,256]{2,1,0:T(2,128)S(1)}, f32[4,2,256]{2,1,0:T(2,128)}, u32[]{:S(2)}) copy-start(f32[4,2,256]{2,1,0:T(2,128)} %param.37) | copy-start | bytes 24580
  0.7 15.8 %copy-start.3 = (bf16[128,1024]{1,0:T(8,128)(2,1)S(1)}, bf16[128,1024]{1,0:T(8,128)(2,1)}, u32[]{:S(2)}) copy-start(bf16[128,1024]{1,0:T(8,128)(2,1)} %param.31) | copy-start | bytes 786436
  0.7 21.9 %copy-start.16 = (f32[16]{0:T(128)S(1)}, f32[16]{0:T(128)}, u32[]{:S(2)}) copy-start(f32[16]{0:T(128)} %param.39) | copy-start | bytes 196
  0.7 21.9 %copy-start.13 = (f32[16]{0:T(128)S(1)}, f32[16]{0:T(128)}, u32[]{:S(2)}) copy-start(f32[16]{0:T(128)} %param.40) | copy-start | bytes 196
  0.7 22.0 %copy-start.15 = (s32[2,4]{1,0:T(2,128)S(1)}, s32[2,4]{1,0:T(2,128)}, u32[]{:S(2)}) copy-start(s32[2,4]{1,0:T(2,128)} %param.44) | copy-start | bytes 100
  0.7 22.0 %copy-start.17 = (f32[16]{0:T(128)S(1)}, f32[16]{0:T(128)}, u32[]{:S(2)}) copy-start(f32[16]{0:T(128)} %param.38) | copy-start | bytes 196
  0.7 29.8 %copy-start.5 = (bf16[2,3,1024]{2,0,1:T(2,128)(2,1)S(1)}, bf16[2,3,1024]{2,0,1:T(2,128)(2,1)}, u32[]{:S(2)}) copy-start(bf16[2,3,1024]{2,0,1:T(2,128)(2,1)} %param.28) | copy-start | bytes 36868
  0.8 29.8 %copy-start.8 = (f32[4,1024]{1,0:T(4,128)S(1)}, f32[4,1024]{1,0:T(4,128)}, u32[]{:S(2)}) copy-start(f32[4,1024]{1,0:T(4,128)} %param.36) | copy-start | bytes 49156
  0.8 15.7 %all-to-all-start = ((bf16[2,16,128]{2,0,1:T(2,128)(2,1)}), bf16[2,16,128]{2,0,1:T(2,128)(2,1)S(1)}, u32[]{:S(2)}, u32[]{:S(2)}) async-start(bf16[2,16,128]{2,0,1:T(2,128)(2,1)} %bitcast.89), calls=%async_computation | async-start | bytes 16384 | tf_op jit(solution)/shard_map/all_to_all | solution.py:113
  10.1 20.6 %copy-start.1 = (f32[2,16,64,128]{3,2,1,0:T(8,128)S(1)}, f32[2,16,64,128]{3,2,1,0:T(8,128)}, u32[]{:S(2)}) copy-start(f32[2,16,64,128]{3,2,1,0:T(8,128)} %param.27) | copy-start | bytes 3145732
  16.5 16.0 %copy-start.12 = (f32[1024]{0:T(1024)S(1)}, f32[1024]{0:T(1024)}, u32[]{:S(2)}) copy-start(f32[1024]{0:T(1024)} %param.41) | copy-start | bytes 12292
  16.5 16.0 %copy-start.14 = (bf16[2,4]{1,0:T(2,128)(2,1)S(1)}, bf16[2,4]{1,0:T(2,128)(2,1)}, u32[]{:S(2)}) copy-start(bf16[2,4]{1,0:T(2,128)(2,1)} %param.45) | copy-start | bytes 52
  18.6 11.8 %all-to-all-start.1 = ((bf16[16,2,2048]{2,1,0:T(2,128)(2,1)}), bf16[16,2,2048]{2,1,0:T(2,128)(2,1)S(1)}, u32[]{:S(2)}, u32[]{:S(2)}) async-start(bf16[16,2,2048]{2,1,0:T(2,128)(2,1)} %reshape.146), calls=%async_computation.1 | async-start | bytes 262144 | tf_op jit(solution)/shard_map/all_to_all | solution.py:134
  30.8 27.5 %copy-start.7 = (f32[2048]{0:T(1024)S(1)}, f32[2048]{0:T(1024)}, u32[]{:S(2)}) copy-start(f32[2048]{0:T(1024)} %param.43) | copy-start | bytes 24580
  30.8 27.5 %copy-start.9 = (f32[2048]{0:T(1024)S(1)}, f32[2048]{0:T(1024)}, u32[]{:S(2)}) copy-start(f32[2048]{0:T(1024)} %param.51) | copy-start | bytes 24580
  33.4 11.0 %all-to-all-start.2 = ((bf16[32,2,1152]{2,1,0:T(2,128)(2,1)}), bf16[32,2,1152]{2,1,0:T(2,128)(2,1)S(1)}, u32[]{:S(2)}, u32[]{:S(2)}) async-start(bf16[32,2,1152]{2,1,0:T(2,128)(2,1)} %broadcast_in_dim.22), calls=%async_computation.2 | async-start | bytes 294912 | tf_op jit(solution)/shard_map/all_to_all | solution.py:163
  36.0 9.7 %collective-permute-start = (bf16[1024,128]{1,0:T(8,128)(2,1)}, bf16[1024,128]{1,0:T(8,128)(2,1)S(1)}, u32[]{:S(2)}, u32[]{:S(2)}) collective-permute-start(bf16[1024,128]{1,0:T(8,128)(2,1)} %param.42), channel_id=1, source_target_pairs={{0,1},{1,0},{2,3},{3,2},{4,5},{5,4},{6,7},{7,6},{8,9},{9,8},{10,11... | collective-permute-start | bytes 786440 | tf_op jit(solution)/shard_map/ppermute | solution.py:123
  46.5 11.6 %all-to-all-start.3 = ((bf16[16,32,128]{2,1,0:T(8,128)(2,1)}), bf16[16,32,128]{2,1,0:T(8,128)(2,1)S(1)}, u32[]{:S(2)}, u32[]{:S(2)}) async-start(bf16[16,32,128]{2,1,0:T(8,128)(2,1)} %broadcast_in_dim.23), calls=%async_computation.3 | async-start | bytes 262144 | tf_op jit(solution)/shard_map/all_to_all | solution.py:177
  60.6 2.6 %copy-start.2 = (bf16[128,2048]{1,0:T(8,128)(2,1)S(1)}, bf16[128,2048]{1,0:T(8,128)(2,1)}, u32[]{:S(2)}) copy-start(bf16[128,2048]{1,0:T(8,128)(2,1)} %param.50) | copy-start | bytes 1572868
  66.6 10.8 %all-to-all-start.4 = ((bf16[32,2,1024]{2,1,0:T(2,128)(2,1)}), bf16[32,2,1024]{2,1,0:T(2,128)(2,1)S(1)}, u32[]{:S(2)}, u32[]{:S(2)}) async-start(bf16[32,2,1024]{2,1,0:T(2,128)(2,1)} %reshape.153), calls=%async_computation.4 | async-start | bytes 262144 | tf_op jit(solution)/shard_map/all_to_all | solution.py:205

commit v2 on v1

--- a/solution.py
+++ b/solution.py
@@ -1,10 +1,16 @@
+import functools
+
 import jax
 import jax.numpy as jnp
 from jax import lax
+from jax.experimental import pallas as pl
+from jax.experimental.pallas import tpu as pltpu
 from jax.sharding import PartitionSpec as P
 
 GROUPS = 4
 TAIL = 128
+LANES = 128
+WORK = 5 * 10**9
 
 norm_eps = 1e-05
 clamp_limit = 7.0
@@ -70,6 +76,492 @@
     grouped = grouped * lax.rsqrt(jnp.mean(grouped * grouped, axis=-1, keepdims=True) + norm_eps)
     mixer_rows = (grouped.reshape(seq_count, channels) * group_gain).astype(bf16)
     return (mixer_rows, state_out, window_inner[:, 1:], window_proj[:, 1:])
+
+
+def early_kernel(
+    tokens_ref,
+    gain_ref,
+    write_ref,
+    read_ref,
+    step_ref,
+    conv_state_ref,
+    proj_state_ref,
+    kernel_ref,
+    proj_kernel_ref,
+    bias_ref,
+    rate_ref,
+    skip_ref,
+    group_gain_ref,
+    routes_ref,
+    logits_ref,
+    state_ref,
+    rows_ref,
+    vec_ref,
+    tail_ref,
+    proj_out_ref,
+    buf_ref,
+    wait_state,
+):
+    taps = kernel_ref.shape[0]
+    seq, width = tokens_ref.shape
+    heads = bias_ref.shape[1]
+    channels = kernel_ref.shape[1]
+    head_width, state_width = state_ref.shape[2:]
+    groups = write_ref.shape[1] // state_width
+    per_group = heads // groups
+    span = per_group * head_width
+    blocks = channels // LANES
+
+    tok = tokens_ref[...].astype(f32)
+    scale = lax.rsqrt(jnp.sum(tok * tok, axis=1, keepdims=True) / width + norm_eps)
+    normed = (tok * scale * gain_ref[...]).astype(bf16)
+
+    tail_ref[...] = jnp.zeros(tail_ref.shape, f32)
+    top = routes_ref.shape[1]
+    tail_ref[:, 0:top] = routes_ref[...].astype(f32)
+    tail_ref[:, top : 2 * top] = logits_ref[...].astype(f32)
+
+    write = jnp.dot(normed, write_ref[...], preferred_element_type=f32).astype(bf16)
+    read = jnp.dot(normed, read_ref[...], preferred_element_type=f32).astype(bf16)
+    step = lax.dot_general(
+        normed, step_ref[...], (((1,), (1,)), ((), ())), preferred_element_type=f32
+    )
+    step = step + bias_ref[...]
+    dt = jnp.maximum(step, 0.0) + jnp.log1p(jnp.exp(-jnp.abs(step)))
+    decay = jnp.exp(-jnp.exp(rate_ref[...]) * dt)
+
+    for t in range(taps - 2):
+        proj_out_ref[:, t] = proj_state_ref[:, t + 1]
+    for t in range(seq):
+        proj_out_ref[t, taps - 2, 0:1, :] = write[t : t + 1]
+        proj_out_ref[t, taps - 2, 1:2, :] = read[t : t + 1]
+        for i, new in ((0, write), (1, read)):
+            total = new[t : t + 1].astype(f32) * proj_kernel_ref[taps - 1, i : i + 1, :]
+            for j in range(taps - 1):
+                total += (
+                    proj_state_ref[t, j, i : i + 1, :].astype(f32)
+                    * proj_kernel_ref[j, i : i + 1, :]
+                )
+            vec_ref[i, t : t + 1, :] = total * jax.nn.sigmoid(total)
+
+    head = lax.broadcasted_iota(jnp.int32, (heads, channels), 0)
+    chan = lax.broadcasted_iota(jnp.int32, (heads, channels), 1)
+    spread = jnp.where(chan // head_width == head, 1.0, 0.0)
+
+    def wide(v):
+        return jnp.dot(v, spread, precision=highest, preferred_element_type=f32)
+
+    dt_wide = wide(dt)
+    decay_wide = wide(decay)
+    skip_wide = wide(jnp.broadcast_to(skip_ref[...], (seq, heads)))
+
+    def place(index, v):
+        for c in range(blocks):
+            rows_ref[index, c * seq : (c + 1) * seq, :] = v[:, c * LANES : (c + 1) * LANES]
+
+    conv = jnp.zeros((seq, channels), f32)
+    for j in range(taps - 1):
+        conv += conv_state_ref[j].astype(f32) * kernel_ref[j : j + 1, :]
+    place(0, conv)
+    place(1, jnp.broadcast_to(kernel_ref[taps - 1 : taps, :], (seq, channels)))
+
+    wait_state()
+    for t in range(seq):
+        for g in range(groups):
+            cols = slice(g * state_width, (g + 1) * state_width)
+            lanes = slice(g * span, (g + 1) * span)
+            read_vec = vec_ref[1, t : t + 1, cols]
+            read_hi = read_vec.astype(bf16)
+            read_lo = (read_vec - read_hi.astype(f32)).astype(bf16)
+            old = state_ref[t, g * per_group : (g + 1) * per_group].reshape(span, state_width)
+            old_hi = old.astype(bf16)
+            old_lo = (old - old_hi.astype(f32)).astype(bf16)
+
+            def along(x, y):
+                return lax.dot_general(
+                    x, y, (((1,), (1,)), ((), ())), preferred_element_type=f32
+                )
+
+            sums = along(read_hi, old_hi) + along(read_hi, old_lo) + along(read_lo, old_hi)
+            buf_ref[t : t + 1, lanes] = sums
+            meet = jnp.sum(vec_ref[0, t : t + 1, cols] * read_vec, axis=1, keepdims=True)
+            buf_ref[seq + t : seq + t + 1, lanes] = jnp.broadcast_to(meet, (1, span))
+    place(2, decay_wide * buf_ref[0:seq, :])
+    place(3, dt_wide * buf_ref[seq : 2 * seq, :] + skip_wide)
+    place(4, jnp.broadcast_to(group_gain_ref[...], (seq, channels)))
+    place(5, jnp.broadcast_to(scale, (seq, channels)))
+    place(6, dt_wide)
+    place(7, decay_wide)
+
+
+def early_stage(count, *refs):
+    sources, outs = refs[:count], refs[count : count + 4]
+    buf_ref, places, sems = refs[count + 4], refs[count + 5 : -1], refs[-1]
+    copies = [
+        pltpu.make_async_copy(source, place, sems.at[i])
+        for i, (source, place) in enumerate(zip(sources, places))
+    ]
+    for copy in copies:
+        copy.start()
+    for copy in copies[:-1]:
+        copy.wait()
+    early_kernel(*places, *outs, buf_ref, copies[-1].wait)
+
+
+def project_kernel(
+    raw_ref, gain_ref, gate_ref, inner_ref, tail_ref, out_ref, tok_ref, in_ref, buf_ref
+):
+    count, rows, lanes = out_ref.shape
+    seq = tail_ref.shape[0]
+    blocks = gate_ref.shape[1] // lanes
+    in_ref[...] = raw_ref[...].astype(f32)
+    for t in range(seq):
+        tok_ref[t * count : (t + 1) * count, :] = in_ref[pl.ds(t, count, stride=seq), :]
+    x = (tok_ref[...] * gain_ref[...]).astype(bf16)
+    for i, weight in ((0, gate_ref), (1, inner_ref)):
+        y = jnp.dot(x, weight[...], preferred_element_type=f32)
+        for c in range(blocks):
+            for t in range(seq):
+                buf_ref[pl.ds((i * blocks + c) * seq + t, count, stride=rows), :] = y[
+                    t * count : (t + 1) * count, c * lanes : (c + 1) * lanes
+                ]
+    last = 2 * blocks * seq
+    tail = jnp.concatenate([tail_ref[...], jnp.zeros((rows - last - seq, lanes), f32)], axis=0)
+    for p in range(count):
+        buf_ref[p * rows + last : (p + 1) * rows, :] = tail
+        out_ref[p] = buf_ref[p * rows : (p + 1) * rows, :].astype(bf16)
+
+
+def mixer_kernel(seq, terms_ref, pre_ref, out_ref, conv_ref, inner_ref, tail_ref, buf_ref):
+    count, rows, lanes = terms_ref.shape
+    n_all, half, _ = out_ref.shape
+    total = jnp.zeros((2 * half, lanes), f32)
+    for p in range(count):
+        total += terms_ref[p, 0 : 2 * half, :].astype(f32)
+        buf_ref[p * 8 : (p + 1) * 8, :] = terms_ref[p, 2 * half : 2 * half + 8, :].astype(f32)
+    for t in range(seq):
+        tail_ref[t * count : (t + 1) * count, :] = buf_ref[pl.ds(t, count, stride=8), :]
+    scale = pre_ref[5]
+    gate = (total[0:half] * scale).astype(bf16).astype(f32)
+    inner = (total[half : 2 * half] * scale).astype(bf16).astype(f32)
+    conv = pre_ref[0] + pre_ref[1] * inner
+    conv = conv * jax.nn.sigmoid(conv)
+    conv_ref[...] = conv
+    inner_ref[...] = inner
+    gated = (pre_ref[2] + pre_ref[3] * conv) * (gate * jax.nn.sigmoid(gate))
+    groups = GROUPS // lax.axis_size("tp")
+    span = half // groups
+    for g in range(groups):
+        part = gated[g * span : (g + 1) * span]
+        square = jnp.sum(part * part, axis=1, keepdims=True)
+        square = jnp.broadcast_to(square, (span, lanes))
+        whole = square
+        for k in range(1, span // seq):
+            whole += pltpu.roll(square, k * seq, 0)
+        part = part * lax.rsqrt(whole / (span // seq * lanes) + norm_eps)
+        buf_ref[g * span : (g + 1) * span, :] = part * pre_ref[4, g * span : (g + 1) * span, :]
+    mixed = buf_ref[0:half, :].astype(bf16)
+    for d in range(n_all):
+        out_ref[d] = mixed
+
+
+def hidden_kernel(
+    count, seq, mix_ref, own_ref, other_ref, tok_ref, out_ref, buf_ref, lhs_ref
+):
+    n_all, half, lanes = mix_ref.shape
+    n_tp = n_all // count
+    my_tp = lax.axis_index("tp")
+    for d in range(n_all):
+        buf_ref[d * half : (d + 1) * half, :] = mix_ref[d].astype(f32)
+    blocks = half // seq
+    total = tok_ref[...]
+    for which, weight in ((0, own_ref), (1, other_ref)):
+        core = lax.rem(my_tp + which, n_tp)
+        for c in range(blocks):
+            for t in range(seq):
+                lhs_ref[t * count : (t + 1) * count, c * lanes : (c + 1) * lanes] = buf_ref[
+                    pl.ds(core * half + c * seq + t, count, stride=n_tp * half), :
+                ].astype(bf16)
+        total += jnp.dot(lhs_ref[...], weight[...], preferred_element_type=f32)
+    hidden = total.astype(bf16)
+    for p in range(count):
+        out_ref[p] = hidden
+
+
+def expert_kernel(
+    top,
+    seq,
+    hid_ref,
+    tail_ref,
+    gain_ref,
+    dgate_ref,
+    gate_ref,
+    up_ref,
+    down_ref,
+    dup_ref,
+    ddown_ref,
+    out_ref,
+    own_ref,
+    x_ref,
+    h_ref,
+    t_ref,
+):
+    blocks, rows, lanes = hid_ref.shape
+    count = rows // seq
+    my_ep = lax.axis_index("ep")
+    own = lax.axis_index("tp") * count + my_ep
+    total = jnp.zeros((rows, lanes), f32)
+    for k in range(blocks):
+        h = hid_ref[k].astype(f32)
+        h_ref[k * rows : (k + 1) * rows, :] = h
+        total += h * h
+    scale = lax.rsqrt(jnp.sum(total, axis=1, keepdims=True) / (blocks * lanes) + norm_eps)
+    dense = jnp.zeros((rows, lanes), f32)
+    for k in range(blocks):
+        h = h_ref[k * rows : (k + 1) * rows, :]
+        x = (h * scale * gain_ref[k : k + 1, :]).astype(bf16)
+        x_ref[:, k * lanes : (k + 1) * lanes] = x
+        dense += x.astype(f32) * dgate_ref[k : k + 1, :]
+    own_ref[...] = h_ref[pl.ds(own, blocks, stride=rows), :]
+    dense_weight = jax.nn.sigmoid(jnp.sum(dense, axis=1, keepdims=True))
+
+    tail = tail_ref[...]
+    lane = lax.broadcasted_iota(jnp.int32, tail.shape, 1)
+    scored = (lane >= top) & (lane < 2 * top)
+    peak = jnp.max(jnp.where(scored, tail, -3e38), axis=1, keepdims=True)
+    raised = jnp.where(scored, jnp.exp(jnp.minimum(tail - peak, 0.0)), 0.0)
+    hits = (lane < top) & (tail.astype(jnp.int32) == my_ep)
+    picked = jnp.where(hits, pltpu.roll(raised, lanes - top, 1), 0.0)
+    row_weight = jnp.sum(picked, axis=1, keepdims=True) / jnp.sum(raised, axis=1, keepdims=True)
+
+    x = x_ref[...]
+    gate = jnp.dot(x, gate_ref[...], preferred_element_type=f32)
+    up = jnp.dot(x, up_ref[...], preferred_element_type=f32)
+    act = (clamped_unit(gate, up) * row_weight).astype(bf16)
+    inner = jnp.dot(x, dup_ref[...], preferred_element_type=f32)
+    dact = (inner * jax.nn.sigmoid(inner) * dense_weight).astype(bf16)
+    for k in range(blocks):
+        cols = slice(k * lanes, (k + 1) * lanes)
+        y = jnp.dot(act, down_ref[:, cols], preferred_element_type=f32) + jnp.dot(
+            dact, ddown_ref[:, cols], preferred_element_type=f32
+        )
+        for t in range(seq):
+            t_ref[pl.ds(t * blocks + k, count, stride=seq * blocks), :] = y[
+                t * count : (t + 1) * count
+            ]
+    for r in range(rows):
+        out_ref[r] = t_ref[r * blocks : (r + 1) * blocks, :].astype(bf16)
+
+
+def call(kernel, name, outs, args, scratch, limit, anywhere=(), sems=0, work=None):
+    vmem = pl.BlockSpec(memory_space=pltpu.VMEM)
+    hbm = pl.BlockSpec(memory_space=pltpu.HBM)
+    args = [
+        pltpu.with_memory_space_constraint(v, pltpu.HBM) if i in anywhere else v
+        for i, v in enumerate(args)
+    ]
+    return pl.pallas_call(
+        kernel,
+        name=name,
+        out_shape=tuple(jax.ShapeDtypeStruct(shape, kind) for shape, kind in outs),
+        in_specs=[hbm if i in anywhere else vmem for i in range(len(args))],
+        out_specs=tuple(vmem for _ in outs),
+        scratch_shapes=[pltpu.VMEM(shape, kind) for shape, kind in scratch]
+        + ([pltpu.SemaphoreType.DMA((sems,))] if sems else []),
+        cost_estimate=work and pl.CostEstimate(
+            flops=work, bytes_accessed=2**20, transcendentals=0
+        ),
+        compiler_params=pltpu.CompilerParams(vmem_limit_bytes=limit * 2**20),
+    )(*args)
+
+
+def final_kernel(terms_ref, own_ref, out_ref):
+    count, blocks, lanes = terms_ref.shape
+    total = own_ref[...]
+    for r in range(count):
+        total += terms_ref[r].astype(f32)
+    for k in range(blocks):
+        out_ref[:, k * lanes : (k + 1) * lanes] = total[k : k + 1, :].astype(bf16)
+
+
+def final_stage(terms, own):
+    count, blocks, lanes = terms.shape
+    vmem = pl.BlockSpec(memory_space=pltpu.VMEM)
+    return pl.pallas_call(
+        final_kernel,
+        name="final_stage",
+        out_shape=jax.ShapeDtypeStruct((1, blocks * lanes), bf16),
+        in_specs=[vmem] * 2,
+        out_specs=vmem,
+        compiler_params=pltpu.CompilerParams(vmem_limit_bytes=4 * 2**20),
+    )(terms, own)
+
+
+def direct(
+    tokens,
+    head_state,
+    conv_state,
+    conv_proj_state,
+    first_gain,
+    gate_weight,
+    inner_weight,
+    write_weight,
+    read_weight,
+    step_weight,
+    conv_kernel,
+    conv_proj_kernel,
+    step_bias,
+    log_rate,
+    skip_gain,
+    group_gain,
+    out_weight,
+    second_gain,
+    routes,
+    route_logits,
+    expert_gate,
+    expert_up,
+    expert_down,
+    dense_up,
+    dense_down,
+    dense_gate,
+):
+    n_ep = lax.axis_size("ep")
+    n_tp = lax.axis_size("tp")
+    n_all = n_ep * n_tp
+    my_ep = lax.axis_index("ep")
+    seq, width = tokens.shape
+    rows = seq * n_ep
+    channels = gate_weight.shape[1]
+    half = channels // LANES * seq
+    taps = conv_kernel.shape[0]
+    heads = step_weight.shape[1]
+    state_cols = write_weight.shape[1]
+    top = routes.shape[1]
+    head_width, state_width = head_state.shape[2:]
+    groups = state_cols // state_width
+
+    raw = lax.all_to_all(tokens, "ep", split_axis=1, concat_axis=0, tiled=True)
+
+    other_weight = lax.ppermute(out_weight, "tp", [(i, (i + 1) % n_tp) for i in range(n_tp)])
+    gain_block = lax.dynamic_slice_in_dim(first_gain, my_ep * LANES, LANES, 0)
+    operands = (
+        tokens,
+        first_gain.reshape(1, width),
+        write_weight,
+        read_weight,
+        step_weight.T,
+        conv_state.transpose(1, 0, 2),
+        conv_proj_state,
+        conv_kernel,
+        conv_proj_kernel,
+        step_bias.reshape(1, heads),
+        log_rate.reshape(1, heads),
+        skip_gain.reshape(1, heads),
+        group_gain.reshape(1, channels),
+        routes,
+        route_logits,
+        head_state,
+    )
+    early, vectors, tail, proj_out = call(
+        functools.partial(early_stage, len(operands)),
+        "early",
+        (
+            ((8, half, LANES), f32),
+            ((2, seq, state_cols), f32),
+            ((seq, LANES), f32),
+            (conv_proj_state.shape, bf16),
+        ),
+        operands,
+        (((2 * seq, channels), f32), *((v.shape, v.dtype) for v in operands)),
+        10,
+        range(len(operands)),
+        len(operands),
+    )
+
+    raw, other_weight = lax.optimization_barrier((raw, other_weight))
+    terms, tok_block = call(
+        project_kernel,
+        "project",
+        (((n_ep, 2 * half + 8, LANES), bf16), ((rows, LANES), f32)),
+        (raw, gain_block.reshape(1, LANES), gate_weight, inner_weight, tail),
+        (((rows, LANES), f32), ((n_ep * (2 * half + 8), LANES), f32)),
+        6,
+        work=WORK,
+    )
+    terms = lax.all_to_all(terms, "ep", split_axis=0, concat_axis=0, tiled=True)
+
+    mixed, conv, inner, tails = call(
+        functools.partial(mixer_kernel, seq),
+        "mixer",
+        (
+            ((n_all, half, LANES), bf16),
+            ((half, LANES), f32),
+            ((half, LANES), f32),
+            ((rows, LANES), f32),
+        ),
+        (terms, early),
+        (((max(n_ep * 8, half), LANES), f32),),
+        4,
+        work=WORK,
+    )
+    mixed = lax.all_to_all(mixed, ("ep", "tp"), split_axis=0, concat_axis=0, tiled=True)
+
+    (hidden,) = call(
+        functools.partial(hidden_kernel, n_ep, seq),
+        "hidden",
+        (((n_ep, rows, LANES), bf16),),
+        (mixed, out_weight, other_weight, tok_block),
+        (((n_all * half, LANES), f32), ((rows, channels), bf16)),
+        6,
+        work=WORK,
+    )
+    hidden = lax.all_to_all(hidden, "ep", split_axis=0, concat_axis=0, tiled=True)
+
+    terms, own_row = call(
+        functools.partial(expert_kernel, top, seq),
+        "experts",
+        (((rows, n_ep, LANES), bf16), ((n_ep, LANES), f32)),
+        (
+            hidden,
+            tails,
+            second_gain.reshape(n_ep, LANES),
+            dense_gate.reshape(n_ep, LANES),
+            expert_gate[0],
+            expert_up[0],
+            expert_down[0],
+            dense_up,
+            dense_down,
+        ),
+        (
+            ((rows, width), bf16),
+            ((rows * n_ep, LANES), f32),
+            ((rows * n_ep, LANES), f32),
+        ),
+        6,
+    )
+    terms = lax.all_to_all(terms, ("ep", "tp"), split_axis=0, concat_axis=0, tiled=True)
+
+    conv, inner, early, vectors, own_row, conv_state, head_state = lax.optimization_barrier(
+        (conv, inner, early, vectors, own_row, conv_state, head_state)
+    )
+
+    def by_head(v):
+        v = v.reshape(channels // LANES, seq, LANES // head_width, head_width)
+        return v.transpose(1, 0, 2, 3).reshape(seq, heads, head_width)
+
+    write_heads = jnp.repeat(
+        vectors[0].reshape(seq, groups, state_width), heads // groups, axis=1
+    )
+    state_out = (
+        by_head(early[7])[:, :, :, None] * head_state
+        + by_head(early[6] * conv)[:, :, :, None] * write_heads[:, :, None, :]
+    )
+    inner_rows = inner.reshape(channels // LANES, seq, LANES).transpose(1, 0, 2)
+    inner_rows = inner_rows.reshape(seq, 1, channels).astype(bf16)
+    conv_out = jnp.concatenate([conv_state[:, 1:], inner_rows], axis=1)
+
+    layer_out = final_stage(terms, own_row)
+    return (layer_out, state_out, conv_out, proj_out)
 
 
 def local(
@@ -110,6 +602,36 @@
     half = gate_weight.shape[1]
     block = gate_weight.shape[0]
 
+    if block == LANES and n_all == rows and half % LANES == 0:
+        return direct(
+            tokens,
+            head_state,
+            conv_state,
+            conv_proj_state,
+            first_gain,
+            gate_weight,
+            inner_weight,
+            write_weight,
+            read_weight,
+            step_weight,
+            conv_kernel,
+            conv_proj_kernel,
+            step_bias,
+            log_rate,
+            skip_gain,
+            group_gain,
+            out_weight,
+            second_gain,
+            routes,
+            route_logits,
+            expert_gate,
+            expert_up,
+            expert_down,
+            dense_up,
+            dense_down,
+            dense_gate,
+        )
+
     raw_block = lax.all_to_all(tokens, "ep", split_axis=1, concat_axis=0, tiled=True)
 
     tok = tokens.astype(f32)

time: 79.1 us -> 64.5 us (0.82)
  blocking collectives: 0 us -> 33.1 us
  waiting for transfers between devices: 32.2 us -> 8.68 us
  matrix products: 12.9 us -> 0 us
  starting transfers between devices: 21.3 us -> 11.1 us
  Pallas kernels: 0 us -> 7.15 us
  local copies, waits for them, and re-layouts: 5 us -> 1.03 us
  other arithmetic: 5.88 us -> 2.21 us
    all_to_all x0 -> x3, blocking collectives: none -> 33.1 us  [the longest x1 11.7 us: direct(): terms = lax.all_to_all(terms, 'ep', split_axis=0, concat_axis=0, tiled=True)]
    all_to_all x5 -> x2, waiting for transfers between devices: 32.2 us -> 8.68 us  [the longest x1 5.72 us: direct(): lax.all_to_all(terms, ('ep', 'tp'), split_axis=0, concat_axis=0, tiled=True)]
    dot_general x10 -> x0, matrix products: 12.9 us -> none  [the longest x1 2.55 us: local(): jnp.dot(activated, expert_down[0], preferred_element_type=f32) * row_weight]
    all_to_all x5 -> x2, starting transfers between devices: 21.1 us -> 10.6 us  [the longest x1 8.01 us: direct(): raw = lax.all_to_all(tokens, 'ep', split_axis=1, concat_axis=0, tiled=True)]
    pallas_call x0 -> x6, Pallas kernels: none -> 7.15 us  [the longest x5 6.5 us: call(): pl.pallas_call(kernel, name=name, out_shape=tuple((jax.ShapeDtypeStruct(s...]
    reduce_sum x11 -> x0, other arithmetic: 3.5 us -> none  [the longest x1 1.38 us: state_step(): jnp.sum(state_out * read_heads[:, :, None, :], axis=-1)]
    add x0 -> x1, other arithmetic: none -> 1.58 us  [direct(): by_head(early[7])[:, :, :, None] * head_state]
    broadcast_in_dim x4 -> x0, local copies, waits for them, and re-layouts: 1.4 us -> none  [the longest x1 0.73 us: local(): packed = jnp.broadcast_to(packed[None], (n_all, seq, half + TAIL))]
  transfers between devices with their start and end apart: 6 -> 3, of which waited for: 5 -> 2; matrix products, arithmetic and copies ran while one was open for 11% -> 5% of each run, Pallas kernels for 0% -> 5%
where the time goes in v2:
time: 64.5 us; the launch traced here: 64.2 us
  blocking collectives  33.1 us (51%)
  starting transfers between devices  11.1 us (17%)
  waiting for transfers between devices  8.68 us (13%)
  Pallas kernels  7.15 us (11%)
  other arithmetic  2.21 us (3%)
  local copies, waits for them, and re-layouts  1.03 us (2%)
  between operations  0.86 us (1%)
    all_to_all x1, blocking collectives, direct(): terms = lax.all_to_all(terms, 'ep', split_axis=0, concat_axis=0, tiled=True)  11.7 us
    all_to_all x1, blocking collectives, direct(): lax.all_to_all(hidden, 'ep', split_axis=0, concat_axis=0, tiled=True)  11.1 us
    all_to_all x1, blocking collectives, direct(): lax.all_to_all(mixed, ('ep', 'tp'), split_axis=0, concat_axis=0, tiled=True)  10.3 us
    all_to_all x1, starting transfers between devices, direct(): raw = lax.all_to_all(tokens, 'ep', split_axis=1, concat_axis=0, tiled=True)  8.01 us
    pallas_call x5, Pallas kernels, call(): pl.pallas_call(kernel, name=name, out_shape=tuple((jax.ShapeDtypeStruct(s...  6.5 us
    all_to_all x1, waiting for transfers between devices, direct(): lax.all_to_all(terms, ('ep', 'tp'), split_axis=0, concat_axis=0, tiled=True)  5.72 us
    all_to_all x1, waiting for transfers between devices, direct(): raw = lax.all_to_all(tokens, 'ep', split_axis=1, concat_axis=0, tiled=True)  2.95 us
    all_to_all x1, starting transfers between devices, direct(): lax.all_to_all(terms, ('ep', 'tp'), split_axis=0, concat_axis=0, tiled=True)  2.56 us
  transfers between devices with their start and end apart: 3, of which 2 were waited for; matrix products, arithmetic and copies ran while one was open for 5% of the time, Pallas kernels for 5%

profile of v2, /device:TPU:0, one launch (start us, length us, event | category | flops | bytes accessed | tf_op | source)
XLA Modules:
  0.0 64.2 jit_solution(2984222844455501417)
XLA Ops:
  0.6 0.0 copy-start.7
  0.6 0.0 copy-start.8
  0.7 0.6 collective-permute-start
  1.2 8.0 %all-to-all-start = ((bf16[2,16,128]{2,0,1:T(2,128)(2,1)}), bf16[2,16,128]{2,0,1:T(2,128)(2,1)S(1)}, u32[]{:S(2)}, u32[]{:S(2)}) async-start(bf16[2,16,128]{2,0,1:T(2,128)(2,1)} %bitcast.43), calls=%async_computation | async-start | bytes 16384 | tf_op jit(solution)/shard_map/all_to_all | solution.py:443
  9.2 0.8 %dynamic-slice_bitcast_fusion.gain_ref = f32[1,128]{1,0:T(1,128)S(1)} fusion(f32[2048]{0:T(1024)} %param.30, s32[]{:T(128)S(6)} %select_n.3), kind=kLoop, calls=%fused_computation.4 | loop fusion | bytes 1028 | tf_op jit(solution)/shard_map/reshape | solution.py:486
  10.0 3.5 %early.1 = (f32[8,16,128]{2,1,0:T(8,128)S(1)}, f32[2,2,256]{2,1,0:T(2,128)S(1)}, f32[2,128]{1,0:T(2,128)S(1)}, bf16[2,3,2,256]{3,2,1,0:T(2,128)(2,1)}) custom-call(bf16[2,2048]{1,0:T(2,128)(2,1)} %refs_0_.1, f32[1,2048]{1,0:T(1,128)} %bitcast.45, bf16[2048,256]{1,0:T(8,128)(2,1)} %refs_2_.1, bf16[2048,256]{1,0:T(8,128)(2,1)} %refs_3_.1, ...), custom_call_target="tpu_custom_call" | custom-call | tf_op jit(solution)/shard_map/early/pallas_call | solution.py:363
  13.5 3.0 %all-to-all-done = bf16[2,16,128]{2,0,1:T(2,128)(2,1)S(1)} async-done(((bf16[2,16,128]{2,0,1:T(2,128)(2,1)}), bf16[2,16,128]{2,0,1:T(2,128)(2,1)S(1)}, u32[]{:S(2)}, u32[]{:S(2)}) %all-to-all-start) | async-done | bytes 8224 | tf_op jit(solution)/shard_map/all_to_all | solution.py:443
  16.5 0.0 collective-permute-done.other_ref
  16.5 0.0 copy-done.7
  16.5 0.0 copy-done.8
  16.5 0.2 project.1
  16.7 11.7 %all_to_all.39.terms_ref = bf16[16,40,128]{2,1,0:T(8,128)(2,1)S(1)} all-to-all(bf16[16,40,128]{2,1,0:T(8,128)(2,1)S(1)} %get-tuple-element.27), channel_id=1, replica_groups=mesh['ep'=16,'tp'=2] {'ep'}, dimensions={0} | all-to-all | bytes 327680 | tf_op jit(solution)/shard_map/all_to_all | solution.py:491
  28.4 0.1 mixer.1
  28.5 10.3 %all_to_all.40.mix_ref = bf16[32,16,128]{2,1,0:T(8,128)(2,1)S(1)} all-to-all(bf16[32,16,128]{2,1,0:T(8,128)(2,1)S(1)} %get-tuple-element.29), channel_id=1, replica_groups=mesh['ep'=16,'tp'=2] {'ep','tp'}, dimensions={0} | all-to-all | bytes 262144 | tf_op jit(solution)/shard_map/all_to_all | solution.py:507
  38.9 0.0 copy-start.3
  38.9 0.0 copy-start.4
  38.9 0.0 copy-start.5
  38.9 0.0 copy-start.6
  38.9 0.4 hidden.1
  39.3 11.1 %all_to_all.41.hid_ref = bf16[16,32,128]{2,1,0:T(8,128)(2,1)S(1)} all-to-all(bf16[16,32,128]{2,1,0:T(8,128)(2,1)S(1)} %hidden.1), channel_id=1, replica_groups=mesh['ep'=16,'tp'=2] {'ep'}, dimensions={0} | all-to-all | bytes 262144 | tf_op jit(solution)/shard_map/all_to_all | solution.py:518
  50.4 0.0 copy-done.1
  50.4 0.0 copy-start.11
  50.4 0.0 copy-start.10
  50.4 2.3 %experts.1 = (bf16[32,16,128]{2,1,0:T(8,128)(2,1)}, f32[16,128]{1,0:T(8,128)S(1)}) custom-call(bf16[16,32,128]{2,1,0:T(8,128)(2,1)S(1)} %all_to_all.41.hid_ref, f32[32,128]{1,0:T(8,128)S(1)} %get-tuple-element.32.tail_ref, f32[16,128]{1,0:T(8,128)S(1)} %bitcast.36, f32[16,128]{1,0:T(8,128)S(1)} %bitcast.37, bf16[2048,512]{1,0:T(8,128)(2,1)S(1)} %bitcast.33, ...), custom_call_target="tpu_custom_call" | custom-call | tf_op jit(solution)/shard_map/experts/pallas_call | solution.py:363
  52.7 2.6 %all-to-all-start.4 = ((bf16[32,16,128]{2,1,0:T(8,128)(2,1)}), bf16[32,16,128]{2,1,0:T(8,128)(2,1)S(1)}, u32[]{:S(2)}, u32[]{:S(2)}) async-start(bf16[32,16,128]{2,1,0:T(8,128)(2,1)} %get-tuple-element.33), calls=%async_computation.4 | async-start | bytes 262144 | tf_op jit(solution)/shard_map/all_to_all | solution.py:542
  55.4 0.1 reshape.65
  55.5 0.1 reshape_squeeze.6
  55.6 0.0 copy-done.11
  55.6 0.6 pad_maximum_fusion
  56.2 1.6 %multiply_add_fusion = f32[2,16,64,128]{3,2,1,0:T(8,128)} fusion(f32[2,16,64,128]{3,2,1,0:T(8,128)S(1)} %copy-done.10, f32[2,16,128]{2,1,0:T(8,128)S(1)} %broadcast_bitcast_fusion, f32[2,16,64]{2,1,0:T(8,128)S(1)} %bitcast.39, f32[2,16,64]{2,1,0:T(8,128)S(1)} %bitcast.40), kind=kLoop, calls=%fused_computation | loop fusion | flops 786432 | bytes 2129920 | tf_op jit(solution)/shard_map/add | solution.py:556
  57.8 5.7 %all-to-all-done.4.terms_ref = bf16[32,16,128]{2,1,0:T(8,128)(2,1)S(1)} async-done(((bf16[32,16,128]{2,1,0:T(8,128)(2,1)}), bf16[32,16,128]{2,1,0:T(8,128)(2,1)S(1)}, u32[]{:S(2)}, u32[]{:S(2)}) %all-to-all-start.4) | async-done | bytes 131104 | tf_op jit(solution)/shard_map/all_to_all | solution.py:542
  63.5 0.6 %final_stage.1 = bf16[1,2048]{1,0:T(2,128)(2,1)} custom-call(bf16[32,16,128]{2,1,0:T(8,128)(2,1)S(1)} %all-to-all-done.4.terms_ref, f32[16,128]{1,0:T(8,128)S(1)} %get-tuple-element.38.own_ref), custom_call_target="tpu_custom_call" | custom-call | tf_op jit(solution)/shard_map/final_stage/pallas_call | solution.py:390
  (21 shorter events, 0.1 us)
Async XLA Ops:
  0.6 15.8 %copy-start.7 = (bf16[128,1024]{1,0:T(8,128)(2,1)S(1)}, bf16[128,1024]{1,0:T(8,128)(2,1)}, u32[]{:S(2)}) copy-start(bf16[128,1024]{1,0:T(8,128)(2,1)} %gate_ref.1) | copy-start | bytes 786436
  0.6 15.8 %copy-start.8 = (bf16[128,1024]{1,0:T(8,128)(2,1)S(1)}, bf16[128,1024]{1,0:T(8,128)(2,1)}, u32[]{:S(2)}) copy-start(bf16[128,1024]{1,0:T(8,128)(2,1)} %inner_ref.1) | copy-start | bytes 786436
  0.7 15.8 %collective-permute-start = (bf16[1024,128]{1,0:T(8,128)(2,1)}, bf16[1024,128]{1,0:T(8,128)(2,1)S(1)}, u32[]{:S(2)}, u32[]{:S(2)}) collective-permute-start(bf16[1024,128]{1,0:T(8,128)(2,1)} %own_ref.1), channel_id=1, source_target_pairs={{0,1},{1,0},{2,3},{3,2},{4,5},{5,4},{6,7},{7,6},{8,9},{9,8},{10,11... | collective-permute-start | bytes 786440 | tf_op jit(solution)/shard_map/ppermute | solution.py:445
  1.2 15.2 %all-to-all-start = ((bf16[2,16,128]{2,0,1:T(2,128)(2,1)}), bf16[2,16,128]{2,0,1:T(2,128)(2,1)S(1)}, u32[]{:S(2)}, u32[]{:S(2)}) async-start(bf16[2,16,128]{2,0,1:T(2,128)(2,1)} %bitcast.43), calls=%async_computation | async-start | bytes 16384 | tf_op jit(solution)/shard_map/all_to_all | solution.py:443
  28.4 10.5 %copy-start.9 = (bf16[1024,128]{1,0:T(8,128)(2,1)S(1)}, bf16[1024,128]{1,0:T(8,128)(2,1)}, u32[]{:S(2)}) copy-start(bf16[1024,128]{1,0:T(8,128)(2,1)} %own_ref.1) | copy-start | bytes 786436
  38.9 11.5 %copy-start = (bf16[1,2048,512]{2,1,0:T(8,128)(2,1)S(1)}, bf16[1,2048,512]{2,1,0:T(8,128)(2,1)}, u32[]{:S(2)}) copy-start(bf16[1,2048,512]{2,1,0:T(8,128)(2,1)} %param.46) | copy-start | bytes 6291460
  38.9 11.5 %copy-start.1 = (bf16[1,2048,512]{2,1,0:T(8,128)(2,1)S(1)}, bf16[1,2048,512]{2,1,0:T(8,128)(2,1)}, u32[]{:S(2)}) copy-start(bf16[1,2048,512]{2,1,0:T(8,128)(2,1)} %param.47) | copy-start | bytes 6291460
  38.9 11.5 %copy-start.2 = (bf16[1,512,2048]{2,1,0:T(8,128)(2,1)S(1)}, bf16[1,512,2048]{2,1,0:T(8,128)(2,1)}, u32[]{:S(2)}) copy-start(bf16[1,512,2048]{2,1,0:T(8,128)(2,1)} %param.48) | copy-start | bytes 6291460
  38.9 11.5 %copy-start.3 = (bf16[2048,128]{1,0:T(8,128)(2,1)S(1)}, bf16[2048,128]{1,0:T(8,128)(2,1)}, u32[]{:S(2)}) copy-start(bf16[2048,128]{1,0:T(8,128)(2,1)} %dup_ref.1) | copy-start | bytes 1572868
  38.9 11.5 %copy-start.4 = (bf16[128,2048]{1,0:T(8,128)(2,1)S(1)}, bf16[128,2048]{1,0:T(8,128)(2,1)}, u32[]{:S(2)}) copy-start(bf16[128,2048]{1,0:T(8,128)(2,1)} %ddown_ref.1) | copy-start | bytes 1572868
  38.9 11.5 %copy-start.5 = (f32[2048]{0:T(1024)S(1)}, f32[2048]{0:T(1024)}, u32[]{:S(2)}) copy-start(f32[2048]{0:T(1024)} %param.43) | copy-start | bytes 24580
  38.9 11.5 %copy-start.6 = (f32[2048]{0:T(1024)S(1)}, f32[2048]{0:T(1024)}, u32[]{:S(2)}) copy-start(f32[2048]{0:T(1024)} %param.51) | copy-start | bytes 24580
  50.4 5.1 %copy-start.11 = (bf16[2,3,1024]{2,0,1:T(2,128)(2,1)S(1)}, bf16[2,3,1024]{2,0,1:T(2,128)(2,1)}, u32[]{:S(2)}) copy-start(bf16[2,3,1024]{2,0,1:T(2,128)(2,1)} %param.28) | copy-start | bytes 36868
  50.4 5.8 %copy-start.10 = (f32[2,16,64,128]{3,2,1,0:T(8,128)S(1)}, f32[2,16,64,128]{3,2,1,0:T(8,128)}, u32[]{:S(2)}) copy-start(f32[2,16,64,128]{3,2,1,0:T(8,128)} %refs_15_.1) | copy-start | bytes 3145732
  52.7 10.8 %all-to-all-start.4 = ((bf16[32,16,128]{2,1,0:T(8,128)(2,1)}), bf16[32,16,128]{2,1,0:T(8,128)(2,1)S(1)}, u32[]{:S(2)}, u32[]{:S(2)}) async-start(bf16[32,16,128]{2,1,0:T(8,128)(2,1)} %get-tuple-element.33), calls=%async_computation.4 | async-start | bytes 262144 | tf_op jit(solution)/shard_map/all_to_all | solution.py:542

commit v3 on v2

--- a/solution.py
+++ b/solution.py
@@ -76,6 +76,10 @@
     grouped = grouped * lax.rsqrt(jnp.mean(grouped * grouped, axis=-1, keepdims=True) + norm_eps)
     mixer_rows = (grouped.reshape(seq_count, channels) * group_gain).astype(bf16)
     return (mixer_rows, state_out, window_inner[:, 1:], window_proj[:, 1:])
+
+
+def open_kernel(out_ref):
+    out_ref[...] = jnp.zeros_like(out_ref)
 
 
 def early_kernel(
@@ -115,20 +119,19 @@
     tok = tokens_ref[...].astype(f32)
     scale = lax.rsqrt(jnp.sum(tok * tok, axis=1, keepdims=True) / width + norm_eps)
     normed = (tok * scale * gain_ref[...]).astype(bf16)
+    write = jnp.dot(normed, write_ref[...], preferred_element_type=f32).astype(bf16)
+    read = jnp.dot(normed, read_ref[...], preferred_element_type=f32).astype(bf16)
+    step = lax.dot_general(
+        normed, step_ref[...], (((1,), (1,)), ((), ())), preferred_element_type=f32
+    )
+    step = step + bias_ref[...]
+    dt = jnp.maximum(step, 0.0) + jnp.log1p(jnp.exp(-jnp.abs(step)))
+    decay = jnp.exp(-jnp.exp(rate_ref[...]) * dt)
 
     tail_ref[...] = jnp.zeros(tail_ref.shape, f32)
     top = routes_ref.shape[1]
     tail_ref[:, 0:top] = routes_ref[...].astype(f32)
     tail_ref[:, top : 2 * top] = logits_ref[...].astype(f32)
-
-    write = jnp.dot(normed, write_ref[...], preferred_element_type=f32).astype(bf16)
-    read = jnp.dot(normed, read_ref[...], preferred_element_type=f32).astype(bf16)
-    step = lax.dot_general(
-        normed, step_ref[...], (((1,), (1,)), ((), ())), preferred_element_type=f32
-    )
-    step = step + bias_ref[...]
-    dt = jnp.maximum(step, 0.0) + jnp.log1p(jnp.exp(-jnp.abs(step)))
-    decay = jnp.exp(-jnp.exp(rate_ref[...]) * dt)
 
     for t in range(taps - 2):
         proj_out_ref[:, t] = proj_state_ref[:, t + 1]
@@ -195,17 +198,11 @@
 
 
 def early_stage(count, *refs):
-    sources, outs = refs[:count], refs[count : count + 4]
-    buf_ref, places, sems = refs[count + 4], refs[count + 5 : -1], refs[-1]
-    copies = [
-        pltpu.make_async_copy(source, place, sems.at[i])
-        for i, (source, place) in enumerate(zip(sources, places))
-    ]
-    for copy in copies:
-        copy.start()
-    for copy in copies[:-1]:
-        copy.wait()
-    early_kernel(*places, *outs, buf_ref, copies[-1].wait)
+    sources, outs = refs[:count], refs[count + 1 : count + 5]
+    buf_ref, state_ref, sems = refs[count + 5 :]
+    copy = pltpu.make_async_copy(sources[-1], state_ref, sems.at[0])
+    copy.start()
+    early_kernel(*sources[:-1], state_ref, *outs, buf_ref, copy.wait)
 
 
 def project_kernel(
@@ -217,7 +214,8 @@
     in_ref[...] = raw_ref[...].astype(f32)
     for t in range(seq):
         tok_ref[t * count : (t + 1) * count, :] = in_ref[pl.ds(t, count, stride=seq), :]
-    x = (tok_ref[...] * gain_ref[...]).astype(bf16)
+    gain = gain_ref[pl.ds(lax.axis_index("ep"), 1), :]
+    x = (tok_ref[...] * gain).astype(bf16)
     for i, weight in ((0, gate_ref), (1, inner_ref)):
         y = jnp.dot(x, weight[...], preferred_element_type=f32)
         for c in range(blocks):
@@ -233,7 +231,7 @@
 
 
 def mixer_kernel(seq, terms_ref, pre_ref, out_ref, conv_ref, inner_ref, tail_ref, buf_ref):
-    count, rows, lanes = terms_ref.shape
+    count, _, lanes = terms_ref.shape
     n_all, half, _ = out_ref.shape
     total = jnp.zeros((2 * half, lanes), f32)
     for p in range(count):
@@ -266,26 +264,26 @@
 
 
 def hidden_kernel(
-    count, seq, mix_ref, own_ref, other_ref, tok_ref, out_ref, buf_ref, lhs_ref
+    count, mix_ref, own_ref, other_ref, tok_ref, out_ref, buf_ref, lhs_ref
 ):
     n_all, half, lanes = mix_ref.shape
     n_tp = n_all // count
     my_tp = lax.axis_index("tp")
     for d in range(n_all):
         buf_ref[d * half : (d + 1) * half, :] = mix_ref[d].astype(f32)
-    blocks = half // seq
-    total = tok_ref[...]
+    blocks = lhs_ref.shape[1] // lanes
+    seq = half // blocks
+    total = tok_ref[pl.ds(pl.multiple_of(my_tp * count, count), count), :]
     for which, weight in ((0, own_ref), (1, other_ref)):
         core = lax.rem(my_tp + which, n_tp)
         for c in range(blocks):
-            for t in range(seq):
-                lhs_ref[t * count : (t + 1) * count, c * lanes : (c + 1) * lanes] = buf_ref[
-                    pl.ds(core * half + c * seq + t, count, stride=n_tp * half), :
-                ].astype(bf16)
+            lhs_ref[:, c * lanes : (c + 1) * lanes] = buf_ref[
+                pl.ds(core * half + c * seq + my_tp, count, stride=n_tp * half), :
+            ].astype(bf16)
         total += jnp.dot(lhs_ref[...], weight[...], preferred_element_type=f32)
     hidden = total.astype(bf16)
-    for p in range(count):
-        out_ref[p] = hidden
+    for d in range(n_all):
+        out_ref[d] = hidden
 
 
 def expert_kernel(
@@ -306,14 +304,17 @@
     h_ref,
     t_ref,
 ):
-    blocks, rows, lanes = hid_ref.shape
-    count = rows // seq
+    count, lanes = hid_ref.shape[1:]
+    rows = count * seq
+    blocks = hid_ref.shape[0] // seq
     my_ep = lax.axis_index("ep")
     own = lax.axis_index("tp") * count + my_ep
     total = jnp.zeros((rows, lanes), f32)
     for k in range(blocks):
-        h = hid_ref[k].astype(f32)
-        h_ref[k * rows : (k + 1) * rows, :] = h
+        for t in range(seq):
+            at = k * rows + t * count
+            h_ref[at : at + count, :] = hid_ref[k * seq + t].astype(f32)
+        h = h_ref[k * rows : (k + 1) * rows, :]
         total += h * h
     scale = lax.rsqrt(jnp.sum(total, axis=1, keepdims=True) / (blocks * lanes) + norm_eps)
     dense = jnp.zeros((rows, lanes), f32)
@@ -353,7 +354,7 @@
         out_ref[r] = t_ref[r * blocks : (r + 1) * blocks, :].astype(bf16)
 
 
-def call(kernel, name, outs, args, scratch, limit, anywhere=(), sems=0, work=None):
+def call(kernel, outs, args, scratch, limit, anywhere=(), sems=0, work=None):
     vmem = pl.BlockSpec(memory_space=pltpu.VMEM)
     hbm = pl.BlockSpec(memory_space=pltpu.HBM)
     args = [
@@ -362,7 +363,6 @@
     ]
     return pl.pallas_call(
         kernel,
-        name=name,
         out_shape=tuple(jax.ShapeDtypeStruct(shape, kind) for shape, kind in outs),
         in_specs=[hbm if i in anywhere else vmem for i in range(len(args))],
         out_specs=tuple(vmem for _ in outs),
@@ -385,7 +385,7 @@
 
 
 def final_stage(terms, own):
-    count, blocks, lanes = terms.shape
+    _, blocks, lanes = terms.shape
     vmem = pl.BlockSpec(memory_space=pltpu.VMEM)
     return pl.pallas_call(
         final_kernel,
@@ -428,12 +428,10 @@
     n_ep = lax.axis_size("ep")
     n_tp = lax.axis_size("tp")
     n_all = n_ep * n_tp
-    my_ep = lax.axis_index("ep")
     seq, width = tokens.shape
     rows = seq * n_ep
     channels = gate_weight.shape[1]
     half = channels // LANES * seq
-    taps = conv_kernel.shape[0]
     heads = step_weight.shape[1]
     state_cols = write_weight.shape[1]
     top = routes.shape[1]
@@ -442,8 +440,9 @@
 
     raw = lax.all_to_all(tokens, "ep", split_axis=1, concat_axis=0, tiled=True)
 
-    other_weight = lax.ppermute(out_weight, "tp", [(i, (i + 1) % n_tp) for i in range(n_tp)])
-    gain_block = lax.dynamic_slice_in_dim(first_gain, my_ep * LANES, LANES, 0)
+    swap = [(i, (i + 1) % n_tp) for i in range(n_tp)]
+    other_weight = lax.ppermute(out_weight, "tp", swap)
+
     operands = (
         tokens,
         first_gain.reshape(1, width),
@@ -462,28 +461,27 @@
         route_logits,
         head_state,
     )
+    (opened,) = call(open_kernel, (((8, LANES), f32),), (), (), 1, work=WORK)
     early, vectors, tail, proj_out = call(
         functools.partial(early_stage, len(operands)),
-        "early",
         (
             ((8, half, LANES), f32),
             ((2, seq, state_cols), f32),
             ((seq, LANES), f32),
             (conv_proj_state.shape, bf16),
         ),
-        operands,
-        (((2 * seq, channels), f32), *((v.shape, v.dtype) for v in operands)),
-        10,
-        range(len(operands)),
-        len(operands),
+        (*operands, opened),
+        (((2 * seq, channels), f32), (head_state.shape, f32)),
+        6,
+        (len(operands) - 1,),
+        1,
     )
 
     raw, other_weight = lax.optimization_barrier((raw, other_weight))
     terms, tok_block = call(
         project_kernel,
-        "project",
         (((n_ep, 2 * half + 8, LANES), bf16), ((rows, LANES), f32)),
-        (raw, gain_block.reshape(1, LANES), gate_weight, inner_weight, tail),
+        (raw, first_gain.reshape(n_ep, LANES), gate_weight, inner_weight, tail),
         (((rows, LANES), f32), ((n_ep * (2 * half + 8), LANES), f32)),
         6,
         work=WORK,
@@ -492,7 +490,6 @@
 
     mixed, conv, inner, tails = call(
         functools.partial(mixer_kernel, seq),
-        "mixer",
         (
             ((n_all, half, LANES), bf16),
             ((half, LANES), f32),
@@ -507,19 +504,17 @@
     mixed = lax.all_to_all(mixed, ("ep", "tp"), split_axis=0, concat_axis=0, tiled=True)
 
     (hidden,) = call(
-        functools.partial(hidden_kernel, n_ep, seq),
-        "hidden",
-        (((n_ep, rows, LANES), bf16),),
+        functools.partial(hidden_kernel, n_ep),
+        (((n_all, n_ep, LANES), bf16),),
         (mixed, out_weight, other_weight, tok_block),
-        (((n_all * half, LANES), f32), ((rows, channels), bf16)),
+        (((n_all * half, LANES), f32), ((n_ep, channels), bf16)),
         6,
         work=WORK,
     )
-    hidden = lax.all_to_all(hidden, "ep", split_axis=0, concat_axis=0, tiled=True)
+    hidden = lax.all_to_all(hidden, ("ep", "tp"), split_axis=0, concat_axis=0, tiled=True)
 
     terms, own_row = call(
         functools.partial(expert_kernel, top, seq),
-        "experts",
         (((rows, n_ep, LANES), bf16), ((n_ep, LANES), f32)),
         (
             hidden,
@@ -602,7 +597,7 @@
     half = gate_weight.shape[1]
     block = gate_weight.shape[0]
 
-    if block == LANES and n_all == rows and half % LANES == 0:
+    if block == LANES and n_all == rows and seq == n_tp and half % LANES == 0:
         return direct(
             tokens,
             head_state,

time: 64.5 us -> 62.5 us (0.969)
  blocking collectives: 33.1 us -> 31.5 us
  Pallas kernels: 7.15 us -> 5.76 us
    pallas_call x5 -> x6, Pallas kernels: 6.5 us -> 5.11 us  [call(): pl.pallas_call(kernel, out_shape=tuple((jax.ShapeDtypeStruct(shape, kind)...]
    unnamed x24 -> x52, local copies, waits for them, and re-layouts: 0.06 us -> 1.4 us
    all_to_all x1, blocking collectives: 11.1 us -> 10.2 us  [direct(): lax.all_to_all(hidden, ('ep', 'tp'), split_axis=0, concat_axis=0, tiled=T...]
    reshape x1 -> x0, local copies, waits for them, and re-layouts: 0.76 us -> none  [direct(): gain_block.reshape(1, LANES)]
  transfers between devices with their start and end apart: 3 -> 3, of which waited for: 2 -> 2; matrix products, arithmetic and copies ran while one was open for 5% -> 4% of each run, Pallas kernels for 5% -> 3%
where the time goes in v3:
time: 62.5 us; the launch traced here: 62.2 us
  blocking collectives  31.5 us (50%)
  starting transfers between devices  11 us (18%)
  waiting for transfers between devices  9.13 us (15%)
  Pallas kernels  5.76 us (9%)
  other arithmetic  2.21 us (4%)
  local copies, waits for them, and re-layouts  1.6 us (3%)
  between operations  1.05 us (2%)
    all_to_all x1, blocking collectives, direct(): terms = lax.all_to_all(terms, 'ep', split_axis=0, concat_axis=0, tiled=True)  11.3 us
    all_to_all x1, blocking collectives, direct(): lax.all_to_all(hidden, ('ep', 'tp'), split_axis=0, concat_axis=0, tiled=T...  10.2 us
    all_to_all x1, blocking collectives, direct(): lax.all_to_all(mixed, ('ep', 'tp'), split_axis=0, concat_axis=0, tiled=True)  10 us
    all_to_all x1, starting transfers between devices, direct(): raw = lax.all_to_all(tokens, 'ep', split_axis=1, concat_axis=0, tiled=True)  8.35 us
    all_to_all x1, waiting for transfers between devices, direct(): lax.all_to_all(terms, ('ep', 'tp'), split_axis=0, concat_axis=0, tiled=True)  5.73 us
    pallas_call x6, Pallas kernels, call(): pl.pallas_call(kernel, out_shape=tuple((jax.ShapeDtypeStruct(shape, kind)...  5.11 us
    all_to_all x1, waiting for transfers between devices, direct(): raw = lax.all_to_all(tokens, 'ep', split_axis=1, concat_axis=0, tiled=True)  3.4 us
    all_to_all x1, starting transfers between devices, direct(): lax.all_to_all(terms, ('ep', 'tp'), split_axis=0, concat_axis=0, tiled=True)  2.56 us
  transfers between devices with their start and end apart: 3, of which 2 were waited for; matrix products, arithmetic and copies ran while one was open for 4% of the time, Pallas kernels for 3%

profile of v3, /device:TPU:0, one launch (start us, length us, event | category | flops | bytes accessed | tf_op | source)
XLA Modules:
  0.0 62.2 jit_solution(5209581067452788290)
XLA Ops:
  0.6 8.4 %all-to-all-start = ((bf16[2,16,128]{2,0,1:T(2,128)(2,1)}), bf16[2,16,128]{2,0,1:T(2,128)(2,1)S(1)}, u32[]{:S(2)}, u32[]{:S(2)}) async-start(bf16[2,16,128]{2,0,1:T(2,128)(2,1)} %bitcast.37), calls=%async_computation | async-start | bytes 16384 | tf_op jit(solution)/shard_map/all_to_all | solution.py:441
  9.0 0.0 copy-start.3
  9.0 0.0 copy-start.7
  9.0 0.0 copy-start.8
  9.1 0.0 copy-start.11
  9.1 0.0 copy-start.12
  9.1 0.0 copy-start.17
  9.1 0.0 copy-start.18
  9.2 0.0 copy-start.21
  9.2 0.1 collective-permute-start
  9.3 0.0 copy-start.22
  9.3 0.0 copy-start.23
  9.3 0.9 %copy-done.3 = bf16[2048,256]{1,0:T(8,128)(2,1)S(1)} copy-done((bf16[2048,256]{1,0:T(8,128)(2,1)S(1)}, bf16[2048,256]{1,0:T(8,128)(2,1)}, u32[]{:S(2)}) %copy-start.3) | copy-done | bytes 1048600
  10.2 0.3 copy-done.4
  10.6 2.2 %shard_map.274 = (f32[8,16,128]{2,1,0:T(8,128)S(1)}, f32[2,2,256]{2,1,0:T(2,128)S(1)}, f32[2,128]{1,0:T(2,128)S(1)}, bf16[2,3,2,256]{3,2,1,0:T(2,128)(2,1)}) custom-call(bf16[2,2048]{1,0:T(2,128)(2,1)S(1)} %copy-done.9, f32[1,2048]{1,0:T(1,128)S(1)} %bitcast.38, bf16[2048,256]{1,0:T(8,128)(2,1)S(1)} %copy-done.3, bf16[2048,256]{1,0:T(8,128)(2,1)S(1)} %copy-done.4, ...), custom_call_target="tpu_custom_call" | custom-call | tf_op jit(solution)/shard_map/pallas_call | solution.py:364
  12.8 3.4 %all-to-all-done = bf16[2,16,128]{2,0,1:T(2,128)(2,1)S(1)} async-done(((bf16[2,16,128]{2,0,1:T(2,128)(2,1)}), bf16[2,16,128]{2,0,1:T(2,128)(2,1)S(1)}, u32[]{:S(2)}, u32[]{:S(2)}) %all-to-all-start) | async-done | bytes 8224 | tf_op jit(solution)/shard_map/all_to_all | solution.py:441
  16.2 0.2 shard_map.275
  16.5 11.3 %all_to_all.39.terms_ref = bf16[16,40,128]{2,1,0:T(8,128)(2,1)S(1)} all-to-all(bf16[16,40,128]{2,1,0:T(8,128)(2,1)S(1)} %get-tuple-element.27), channel_id=1, replica_groups=mesh['ep'=16,'tp'=2] {'ep'}, dimensions={0} | all-to-all | bytes 327680 | tf_op jit(solution)/shard_map/all_to_all | solution.py:489
  27.7 0.1 shard_map.276
  27.9 10.0 %all_to_all.40.mix_ref = bf16[32,16,128]{2,1,0:T(8,128)(2,1)S(1)} all-to-all(bf16[32,16,128]{2,1,0:T(8,128)(2,1)S(1)} %get-tuple-element.29), channel_id=1, replica_groups=mesh['ep'=16,'tp'=2] {'ep','tp'}, dimensions={0} | all-to-all | bytes 262144 | tf_op jit(solution)/shard_map/all_to_all | solution.py:504
  37.9 0.0 copy-start.13
  37.9 0.0 copy-start.14
  38.0 0.3 shard_map.277
  38.2 10.2 %all_to_all.41.hid_ref = bf16[32,16,128]{2,1,0:T(8,128)(2,1)S(1)} all-to-all(bf16[32,16,128]{2,1,0:T(8,128)(2,1)S(1)} %shard_map.277), channel_id=1, replica_groups=mesh['ep'=16,'tp'=2] {'ep','tp'}, dimensions={0} | all-to-all | bytes 262144 | tf_op jit(solution)/shard_map/all_to_all | solution.py:514
  48.5 2.3 %shard_map.278 = (bf16[32,16,128]{2,1,0:T(8,128)(2,1)}, f32[16,128]{1,0:T(8,128)S(1)}) custom-call(bf16[32,16,128]{2,1,0:T(8,128)(2,1)S(1)} %all_to_all.41.hid_ref, f32[32,128]{1,0:T(8,128)S(1)} %get-tuple-element.32.tail_ref, f32[16,128]{1,0:T(8,128)S(1)} %bitcast.40, f32[16,128]{1,0:T(8,128)S(1)} %bitcast.41, bf16[2048,512]{1,0:T(8,128)(2,1)S(1)} %bitcast.32, ...), custom_call_target="tpu_custom_call" | custom-call | tf_op jit(solution)/shard_map/pallas_call | solution.py:364
  50.8 2.6 %all-to-all-start.4 = ((bf16[32,16,128]{2,1,0:T(8,128)(2,1)}), bf16[32,16,128]{2,1,0:T(8,128)(2,1)S(1)}, u32[]{:S(2)}, u32[]{:S(2)}) async-start(bf16[32,16,128]{2,1,0:T(8,128)(2,1)} %get-tuple-element.33), calls=%async_computation.4 | async-start | bytes 262144 | tf_op jit(solution)/shard_map/all_to_all | solution.py:537
  53.4 0.1 reshape.65
  53.5 0.1 reshape_squeeze.6
  53.6 0.6 pad_maximum_fusion
  54.2 1.6 %multiply_add_fusion = f32[2,16,64,128]{3,2,1,0:T(8,128)} fusion(f32[2,16,64,128]{3,2,1,0:T(8,128)S(1)} %copy-done.25, f32[2,16,128]{2,1,0:T(8,128)S(1)} %broadcast_bitcast_fusion, f32[2,16,64]{2,1,0:T(8,128)S(1)} %bitcast.47, f32[2,16,64]{2,1,0:T(8,128)S(1)} %bitcast.48), kind=kLoop, calls=%fused_computation | loop fusion | flops 786432 | bytes 2129920 | tf_op jit(solution)/shard_map/add | solution.py:551
  55.8 5.7 %all-to-all-done.4.terms_ref = bf16[32,16,128]{2,1,0:T(8,128)(2,1)S(1)} async-done(((bf16[32,16,128]{2,1,0:T(8,128)(2,1)}), bf16[32,16,128]{2,1,0:T(8,128)(2,1)S(1)}, u32[]{:S(2)}, u32[]{:S(2)}) %all-to-all-start.4) | async-done | bytes 131104 | tf_op jit(solution)/shard_map/all_to_all | solution.py:537
  61.6 0.6 %final_stage.1 = bf16[1,2048]{1,0:T(2,128)(2,1)} custom-call(bf16[32,16,128]{2,1,0:T(8,128)(2,1)S(1)} %all-to-all-done.4.terms_ref, f32[16,128]{1,0:T(8,128)S(1)} %get-tuple-element.38.own_ref), custom_call_target="tpu_custom_call" | custom-call | tf_op jit(solution)/shard_map/final_stage/pallas_call | solution.py:390
  (49 shorter events, 0.2 us)
Async XLA Ops:
  0.6 15.6 %all-to-all-start = ((bf16[2,16,128]{2,0,1:T(2,128)(2,1)}), bf16[2,16,128]{2,0,1:T(2,128)(2,1)S(1)}, u32[]{:S(2)}, u32[]{:S(2)}) async-start(bf16[2,16,128]{2,0,1:T(2,128)(2,1)} %bitcast.37), calls=%async_computation | async-start | bytes 16384 | tf_op jit(solution)/shard_map/all_to_all | solution.py:441
  9.0 1.2 %copy-start.3 = (bf16[2048,256]{1,0:T(8,128)(2,1)S(1)}, bf16[2048,256]{1,0:T(8,128)(2,1)}, u32[]{:S(2)}) copy-start(bf16[2048,256]{1,0:T(8,128)(2,1)} %refs_2_.1) | copy-start | bytes 3145732
  9.0 1.5 %copy-start.4 = (bf16[2048,256]{1,0:T(8,128)(2,1)S(1)}, bf16[2048,256]{1,0:T(8,128)(2,1)}, u32[]{:S(2)}) copy-start(bf16[2048,256]{1,0:T(8,128)(2,1)} %refs_3_.1) | copy-start | bytes 3145732
  9.0 1.5 %copy-start.7 = (bf16[2048,16]{0,1:T(8,128)(2,1)S(1)}, bf16[2048,16]{0,1:T(8,128)(2,1)}, u32[]{:S(2)}) copy-start(bf16[2048,16]{0,1:T(8,128)(2,1)} %param.35) | copy-start | bytes 196612
  9.0 1.5 %copy-start.8 = (bf16[2,3,1024]{2,0,1:T(2,128)(2,1)S(1)}, bf16[2,3,1024]{2,0,1:T(2,128)(2,1)}, u32[]{:S(2)}) copy-start(bf16[2,3,1024]{2,0,1:T(2,128)(2,1)} %param.28) | copy-start | bytes 36868
  9.0 1.5 %copy-start.9 = (bf16[2,2048]{1,0:T(2,128)(2,1)S(1)}, bf16[2,2048]{1,0:T(2,128)(2,1)}, u32[]{:S(2)}) copy-start(bf16[2,2048]{1,0:T(2,128)(2,1)} %refs_0_.1) | copy-start | bytes 24580
  9.0 1.5 %copy-start.10 = (f32[4,1024]{1,0:T(4,128)S(1)}, f32[4,1024]{1,0:T(4,128)}, u32[]{:S(2)}) copy-start(f32[4,1024]{1,0:T(4,128)} %refs_7_.1) | copy-start | bytes 49156
  9.1 1.5 %copy-start.11 = (f32[4,2,256]{2,1,0:T(2,128)S(1)}, f32[4,2,256]{2,1,0:T(2,128)}, u32[]{:S(2)}) copy-start(f32[4,2,256]{2,1,0:T(2,128)} %refs_8_.1) | copy-start | bytes 24580
  9.1 1.5 %copy-start.12 = (f32[2048]{0:T(1024)S(1)}, f32[2048]{0:T(1024)}, u32[]{:S(2)}) copy-start(f32[2048]{0:T(1024)} %param.30) | copy-start | bytes 24580
  9.1 1.5 %copy-start.15 = (bf16[2,3,2,256]{3,2,1,0:T(2,128)(2,1)S(1)}, bf16[2,3,2,256]{3,2,1,0:T(2,128)(2,1)}, u32[]{:S(2)}) copy-start(bf16[2,3,2,256]{3,2,1,0:T(2,128)(2,1)} %refs_6_.1) | copy-start | bytes 18436
  9.1 1.5 %copy-start.16 = (f32[1024]{0:T(1024)S(1)}, f32[1024]{0:T(1024)}, u32[]{:S(2)}) copy-start(f32[1024]{0:T(1024)} %param.41) | copy-start | bytes 12292
  9.1 1.5 %copy-start.17 = (s32[2,4]{1,0:T(2,128)S(1)}, s32[2,4]{1,0:T(2,128)}, u32[]{:S(2)}) copy-start(s32[2,4]{1,0:T(2,128)} %refs_13_.1) | copy-start | bytes 100
  9.1 1.5 %copy-start.18 = (f32[16]{0:T(128)S(1)}, f32[16]{0:T(128)}, u32[]{:S(2)}) copy-start(f32[16]{0:T(128)} %param.38) | copy-start | bytes 196
  9.1 1.5 %copy-start.19 = (f32[16]{0:T(128)S(1)}, f32[16]{0:T(128)}, u32[]{:S(2)}) copy-start(f32[16]{0:T(128)} %param.39) | copy-start | bytes 196
  9.1 1.5 %copy-start.20 = (f32[16]{0:T(128)S(1)}, f32[16]{0:T(128)}, u32[]{:S(2)}) copy-start(f32[16]{0:T(128)} %param.40) | copy-start | bytes 196
  9.2 1.5 %copy-start.21 = (bf16[2,4]{1,0:T(2,128)(2,1)S(1)}, bf16[2,4]{1,0:T(2,128)(2,1)}, u32[]{:S(2)}) copy-start(bf16[2,4]{1,0:T(2,128)(2,1)} %refs_14_.1) | copy-start | bytes 52
  9.2 7.0 %collective-permute-start = (bf16[1024,128]{1,0:T(8,128)(2,1)}, bf16[1024,128]{1,0:T(8,128)(2,1)S(1)}, u32[]{:S(2)}, u32[]{:S(2)}) collective-permute-start(bf16[1024,128]{1,0:T(8,128)(2,1)} %own_ref.1), channel_id=1, source_target_pairs={{0,1},{1,0},{2,3},{3,2},{4,5},{5,4},{6,7},{7,6},{8,9},{9,8},{10,11... | collective-permute-start | bytes 786440 | tf_op jit(solution)/shard_map/ppermute | solution.py:444
  9.3 7.0 %copy-start.22 = (bf16[128,1024]{1,0:T(8,128)(2,1)S(1)}, bf16[128,1024]{1,0:T(8,128)(2,1)}, u32[]{:S(2)}) copy-start(bf16[128,1024]{1,0:T(8,128)(2,1)} %gate_ref.1) | copy-start | bytes 786436
  9.3 6.9 %copy-start.23 = (bf16[128,1024]{1,0:T(8,128)(2,1)S(1)}, bf16[128,1024]{1,0:T(8,128)(2,1)}, u32[]{:S(2)}) copy-start(bf16[128,1024]{1,0:T(8,128)(2,1)} %inner_ref.1) | copy-start | bytes 786436
  27.7 10.2 %copy-start.24 = (bf16[1024,128]{1,0:T(8,128)(2,1)S(1)}, bf16[1024,128]{1,0:T(8,128)(2,1)}, u32[]{:S(2)}) copy-start(bf16[1024,128]{1,0:T(8,128)(2,1)} %own_ref.1) | copy-start | bytes 786436
  37.9 10.5 %copy-start = (bf16[1,2048,512]{2,1,0:T(8,128)(2,1)S(1)}, bf16[1,2048,512]{2,1,0:T(8,128)(2,1)}, u32[]{:S(2)}) copy-start(bf16[1,2048,512]{2,1,0:T(8,128)(2,1)} %param.46) | copy-start | bytes 6291460
  37.9 10.5 %copy-start.1 = (bf16[1,2048,512]{2,1,0:T(8,128)(2,1)S(1)}, bf16[1,2048,512]{2,1,0:T(8,128)(2,1)}, u32[]{:S(2)}) copy-start(bf16[1,2048,512]{2,1,0:T(8,128)(2,1)} %param.47) | copy-start | bytes 6291460
  37.9 10.5 %copy-start.2 = (bf16[1,512,2048]{2,1,0:T(8,128)(2,1)S(1)}, bf16[1,512,2048]{2,1,0:T(8,128)(2,1)}, u32[]{:S(2)}) copy-start(bf16[1,512,2048]{2,1,0:T(8,128)(2,1)} %param.48) | copy-start | bytes 6291460
  37.9 10.5 %copy-start.5 = (bf16[2048,128]{1,0:T(8,128)(2,1)S(1)}, bf16[2048,128]{1,0:T(8,128)(2,1)}, u32[]{:S(2)}) copy-start(bf16[2048,128]{1,0:T(8,128)(2,1)} %dup_ref.1) | copy-start | bytes 1572868
  37.9 10.5 %copy-start.6 = (bf16[128,2048]{1,0:T(8,128)(2,1)S(1)}, bf16[128,2048]{1,0:T(8,128)(2,1)}, u32[]{:S(2)}) copy-start(bf16[128,2048]{1,0:T(8,128)(2,1)} %ddown_ref.1) | copy-start | bytes 1572868
  37.9 10.5 %copy-start.13 = (f32[2048]{0:T(1024)S(1)}, f32[2048]{0:T(1024)}, u32[]{:S(2)}) copy-start(f32[2048]{0:T(1024)} %param.43) | copy-start | bytes 24580
  37.9 10.5 %copy-start.14 = (f32[2048]{0:T(1024)S(1)}, f32[2048]{0:T(1024)}, u32[]{:S(2)}) copy-start(f32[2048]{0:T(1024)} %param.51) | copy-start | bytes 24580
  48.5 5.8 %copy-start.25 = (f32[2,16,64,128]{3,2,1,0:T(8,128)S(1)}, f32[2,16,64,128]{3,2,1,0:T(8,128)}, u32[]{:S(2)}) copy-start(f32[2,16,64,128]{3,2,1,0:T(8,128)} %refs_15_.1) | copy-start | bytes 3145732
  50.8 10.8 %all-to-all-start.4 = ((bf16[32,16,128]{2,1,0:T(8,128)(2,1)}), bf16[32,16,128]{2,1,0:T(8,128)(2,1)S(1)}, u32[]{:S(2)}, u32[]{:S(2)}) async-start(bf16[32,16,128]{2,1,0:T(8,128)(2,1)} %get-tuple-element.33), calls=%async_computation.4 | async-start | bytes 262144 | tf_op jit(solution)/shard_map/all_to_all | solution.py:537

commit v4 on v3

--- a/solution.py
+++ b/solution.py
@@ -232,7 +232,8 @@
 
 def mixer_kernel(seq, terms_ref, pre_ref, out_ref, conv_ref, inner_ref, tail_ref, buf_ref):
     count, _, lanes = terms_ref.shape
-    n_all, half, _ = out_ref.shape
+    n_all, blocks, _ = out_ref.shape
+    half = blocks * seq
     total = jnp.zeros((2 * half, lanes), f32)
     for p in range(count):
         total += terms_ref[p, 0 : 2 * half, :].astype(f32)
@@ -258,32 +259,77 @@
             whole += pltpu.roll(square, k * seq, 0)
         part = part * lax.rsqrt(whole / (span // seq * lanes) + norm_eps)
         buf_ref[g * span : (g + 1) * span, :] = part * pre_ref[4, g * span : (g + 1) * span, :]
-    mixed = buf_ref[0:half, :].astype(bf16)
-    for d in range(n_all):
-        out_ref[d] = mixed
+    for t in range(seq):
+        mixed = buf_ref[pl.ds(t, blocks, stride=seq), :].astype(bf16)
+        for d in range(t, n_all, seq):
+            out_ref[d] = mixed
 
 
 def hidden_kernel(
     count, mix_ref, own_ref, other_ref, tok_ref, out_ref, buf_ref, lhs_ref
 ):
-    n_all, half, lanes = mix_ref.shape
+    n_all, blocks, lanes = mix_ref.shape
     n_tp = n_all // count
     my_tp = lax.axis_index("tp")
     for d in range(n_all):
-        buf_ref[d * half : (d + 1) * half, :] = mix_ref[d].astype(f32)
-    blocks = lhs_ref.shape[1] // lanes
-    seq = half // blocks
+        buf_ref[d * blocks : (d + 1) * blocks, :] = mix_ref[d].astype(f32)
     total = tok_ref[pl.ds(pl.multiple_of(my_tp * count, count), count), :]
     for which, weight in ((0, own_ref), (1, other_ref)):
         core = lax.rem(my_tp + which, n_tp)
         for c in range(blocks):
             lhs_ref[:, c * lanes : (c + 1) * lanes] = buf_ref[
-                pl.ds(core * half + c * seq + my_tp, count, stride=n_tp * half), :
+                pl.ds(core * blocks + c, count, stride=n_tp * blocks), :
             ].astype(bf16)
         total += jnp.dot(lhs_ref[...], weight[...], preferred_element_type=f32)
     hidden = total.astype(bf16)
     for d in range(n_all):
         out_ref[d] = hidden
+
+
+def new_states(
+    state_ref,
+    conv_ref,
+    inner_ref,
+    pre_ref,
+    vec_ref,
+    old_ref,
+    state_out_ref,
+    conv_out_ref,
+    new_ref,
+    taps_ref,
+    sems,
+):
+    seq, heads, head_width, state_width = state_ref.shape
+    half, lanes = conv_ref.shape
+    taps = taps_ref.shape[0]
+    groups = vec_ref.shape[2] // state_width
+    per_group = heads // groups
+    per_block = lanes // head_width
+    columns = jnp.concatenate([pre_ref[6] * conv_ref[...], pre_ref[7]], axis=0).T
+    copies = []
+    for t in range(seq):
+        for h in range(heads):
+            row = h // per_block * seq + t
+            part = slice(h % per_block * head_width, (h % per_block + 1) * head_width)
+            g = h // per_group
+            write = vec_ref[0, t : t + 1, g * state_width : (g + 1) * state_width]
+            new_ref[t, h] = (
+                columns[part, half + row : half + row + 1] * state_ref[t, h]
+                + columns[part, row : row + 1] * write
+            )
+        copies.append(
+            pltpu.make_async_copy(new_ref.at[t], state_out_ref.at[t], sems.at[t])
+        )
+        copies[-1].start()
+    for j in range(taps - 1):
+        taps_ref[j] = old_ref[j + 1]
+    for c in range(half // seq):
+        taps_ref[taps - 1, :, c * lanes : (c + 1) * lanes] = inner_ref[
+            c * seq : (c + 1) * seq, :
+        ].astype(bf16)
+    copies.append(pltpu.make_async_copy(taps_ref, conv_out_ref, sems.at[seq]))
+    copies[-1].start()
+    return copies
 
 
 def expert_kernel(
@@ -298,12 +344,36 @@
     down_ref,
     dup_ref,
     ddown_ref,
+    state_ref,
+    conv_ref,
+    inner_ref,
+    pre_ref,
+    vec_ref,
+    old_ref,
     out_ref,
     own_ref,
+    state_out_ref,
+    conv_out_ref,
     x_ref,
     h_ref,
     t_ref,
+    new_ref,
+    taps_ref,
+    sems,
 ):
+    copies = new_states(
+        state_ref,
+        conv_ref,
+        inner_ref,
+        pre_ref,
+        vec_ref,
+        old_ref,
+        state_out_ref,
+        conv_out_ref,
+        new_ref,
+        taps_ref,
+        sems,
+    )
     count, lanes = hid_ref.shape[1:]
     rows = count * seq
     blocks = hid_ref.shape[0] // seq
@@ -341,20 +411,24 @@
     act = (clamped_unit(gate, up) * row_weight).astype(bf16)
     inner = jnp.dot(x, dup_ref[...], preferred_element_type=f32)
     dact = (inner * jax.nn.sigmoid(inner) * dense_weight).astype(bf16)
-    for k in range(blocks):
-        cols = slice(k * lanes, (k + 1) * lanes)
+    wide = 4
+    for j in range(blocks // wide):
+        cols = slice(j * wide * lanes, (j + 1) * wide * lanes)
         y = jnp.dot(act, down_ref[:, cols], preferred_element_type=f32) + jnp.dot(
             dact, ddown_ref[:, cols], preferred_element_type=f32
         )
-        for t in range(seq):
-            t_ref[pl.ds(t * blocks + k, count, stride=seq * blocks), :] = y[
-                t * count : (t + 1) * count
-            ]
+        for i in range(wide):
+            for t in range(seq):
+                t_ref[pl.ds(t * blocks + j * wide + i, count, stride=seq * blocks), :] = y[
+                    t * count : (t + 1) * count, i * lanes : (i + 1) * lanes
+                ]
     for r in range(rows):
         out_ref[r] = t_ref[r * blocks : (r + 1) * blocks, :].astype(bf16)
-
-
-def call(kernel, outs, args, scratch, limit, anywhere=(), sems=0, work=None):
+    for copy in copies:
+        copy.wait()
+
+
+def call(kernel, outs, args, scratch, limit, anywhere=(), sems=0, work=None, outside=()):
     vmem = pl.BlockSpec(memory_space=pltpu.VMEM)
     hbm = pl.BlockSpec(memory_space=pltpu.HBM)
     args = [
@@ -365,7 +439,7 @@
         kernel,
         out_shape=tuple(jax.ShapeDtypeStruct(shape, kind) for shape, kind in outs),
         in_specs=[hbm if i in anywhere else vmem for i in range(len(args))],
-        out_specs=tuple(vmem for _ in outs),
+        out_specs=tuple(hbm if i in outside else vmem for i in range(len(outs))),
         scratch_shapes=[pltpu.VMEM(shape, kind) for shape, kind in scratch]
         + ([pltpu.SemaphoreType.DMA((sems,))] if sems else []),
         cost_estimate=work and pl.CostEstimate(
@@ -435,8 +509,6 @@
     heads = step_weight.shape[1]
     state_cols = write_weight.shape[1]
     top = routes.shape[1]
-    head_width, state_width = head_state.shape[2:]
-    groups = state_cols // state_width
 
     raw = lax.all_to_all(tokens, "ep", split_axis=1, concat_axis=0, tiled=True)
 
@@ -491,7 +563,7 @@
     mixed, conv, inner, tails = call(
         functools.partial(mixer_kernel, seq),
         (
-            ((n_all, half, LANES), bf16),
+            ((n_all, half // seq, LANES), bf16),
             ((half, LANES), f32),
             ((half, LANES), f32),
             ((rows, LANES), f32),
@@ -507,15 +579,21 @@
         functools.partial(hidden_kernel, n_ep),
         (((n_all, n_ep, LANES), bf16),),
         (mixed, out_weight, other_weight, tok_block),
-        (((n_all * half, LANES), f32), ((n_ep, channels), bf16)),
+        (((n_all * half // seq, LANES), f32), ((n_ep, channels), bf16)),
         6,
         work=WORK,
     )
     hidden = lax.all_to_all(hidden, ("ep", "tp"), split_axis=0, concat_axis=0, tiled=True)
 
-    terms, own_row = call(
+    old = conv_state.transpose(1, 0, 2)
+    terms, own_row, state_out, conv_out = call(
         functools.partial(expert_kernel, top, seq),
-        (((rows, n_ep, LANES), bf16), ((n_ep, LANES), f32)),
+        (
+            ((rows, n_ep, LANES), bf16),
+            ((n_ep, LANES), f32),
+            (head_state.shape, f32),
+            (old.shape, bf16),
+        ),
         (
             hidden,
             tails,
@@ -526,35 +604,26 @@
             expert_down[0],
             dense_up,
             dense_down,
+            head_state,
+            conv,
+            inner,
+            early,
+            vectors,
+            old,
         ),
         (
             ((rows, width), bf16),
             ((rows * n_ep, LANES), f32),
             ((rows * n_ep, LANES), f32),
+            (head_state.shape, f32),
+            (old.shape, bf16),
         ),
-        6,
+        8,
+        sems=seq + 1,
+        outside=(2, 3),
     )
     terms = lax.all_to_all(terms, ("ep", "tp"), split_axis=0, concat_axis=0, tiled=True)
-
-    conv, inner, early, vectors, own_row, conv_state, head_state = lax.optimization_barrier(
-        (conv, inner, early, vectors, own_row, conv_state, head_state)
-    )
-
-    def by_head(v):
-        v = v.reshape(channels // LANES, seq, LANES // head_width, head_width)
-        return v.transpose(1, 0, 2, 3).reshape(seq, heads, head_width)
-
-    write_heads = jnp.repeat(
-        vectors[0].reshape(seq, groups, state_width), heads // groups, axis=1
-    )
-    state_out = (
-        by_head(early[7])[:, :, :, None] * head_state
-        + by_head(early[6] * conv)[:, :, :, None] * write_heads[:, :, None, :]
-    )
-    inner_rows = inner.reshape(channels // LANES, seq, LANES).transpose(1, 0, 2)
-    inner_rows = inner_rows.reshape(seq, 1, channels).astype(bf16)
-    conv_out = jnp.concatenate([conv_state[:, 1:], inner_rows], axis=1)
-
+    conv_out = conv_out.transpose(1, 0, 2)
     layer_out = final_stage(terms, own_row)
     return (layer_out, state_out, conv_out, proj_out)
 

time: 62.5 us -> 60.7 us (0.971)
  blocking collectives: 31.5 us -> 40.6 us
  waiting for transfers between devices: 9.13 us -> 3.4 us
  starting transfers between devices: 11 us -> 8.42 us
  other arithmetic: 2.21 us -> 0 us
    all_to_all x0 -> x1, blocking collectives: none -> 9.91 us  [direct(): lax.all_to_all(terms, ('ep', 'tp'), split_axis=0, concat_axis=0, tiled=True)]
    all_to_all x1 -> x0, waiting for transfers between devices: 5.73 us -> none  [direct(): lax.all_to_all(terms, ('ep', 'tp'), split_axis=0, concat_axis=0, tiled=True)]
    all_to_all x1 -> x0, starting transfers between devices: 2.56 us -> none  [direct(): lax.all_to_all(terms, ('ep', 'tp'), split_axis=0, concat_axis=0, tiled=True)]
    add x1 -> x0, other arithmetic: 1.59 us -> none  [direct(): by_head(early[7])[:, :, :, None] * head_state]
    all_to_all x1, blocking collectives: 10 us -> 9.24 us  [direct(): lax.all_to_all(mixed, ('ep', 'tp'), split_axis=0, concat_axis=0, tiled=True)]
  transfers between devices with their start and end apart: 3 -> 2, of which waited for: 2 -> 1; matrix products, arithmetic and copies ran while one was open for 4% -> 0% of each run, Pallas kernels for 3% -> 4%
where the time goes in v4:
time: 60.7 us; the launch traced here: 60.4 us
  blocking collectives  40.6 us (67%)
  starting transfers between devices  8.42 us (14%)
  Pallas kernels  5.58 us (9%)
  waiting for transfers between devices  3.4 us (6%)
  local copies, waits for them, and re-layouts  1.4 us (2%)
  between operations  0.99 us (2%)
    all_to_all x1, blocking collectives, direct(): terms = lax.all_to_all(terms, 'ep', split_axis=0, concat_axis=0, tiled=True)  11.3 us
    all_to_all x1, blocking collectives, direct(): lax.all_to_all(hidden, ('ep', 'tp'), split_axis=0, concat_axis=0, tiled=T...  10.2 us
    all_to_all x1, blocking collectives, direct(): lax.all_to_all(terms, ('ep', 'tp'), split_axis=0, concat_axis=0, tiled=True)  9.91 us
    all_to_all x1, blocking collectives, direct(): lax.all_to_all(mixed, ('ep', 'tp'), split_axis=0, concat_axis=0, tiled=True)  9.24 us
    all_to_all x1, starting transfers between devices, direct(): raw = lax.all_to_all(tokens, 'ep', split_axis=1, concat_axis=0, tiled=True)  8.35 us
    pallas_call x6, Pallas kernels, call(): pl.pallas_call(kernel, out_shape=tuple((jax.ShapeDtypeStruct(shape, kind)...  4.94 us
    all_to_all x1, waiting for transfers between devices, direct(): raw = lax.all_to_all(tokens, 'ep', split_axis=1, concat_axis=0, tiled=True)  3.4 us
    unnamed x52, local copies, waits for them, and re-layouts  1.4 us
  transfers between devices with their start and end apart: 2, of which 1 were waited for; matrix products, arithmetic and copies ran while one was open for 0% of the time, Pallas kernels for 4%

profile of v4, /device:TPU:0, one launch (start us, length us, event | category | flops | bytes accessed | tf_op | source)
XLA Modules:
  0.0 60.4 jit_solution(2310271544175734565)
XLA Ops:
  0.6 8.4 %all-to-all-start = ((bf16[2,16,128]{2,0,1:T(2,128)(2,1)}), bf16[2,16,128]{2,0,1:T(2,128)(2,1)S(1)}, u32[]{:S(2)}, u32[]{:S(2)}) async-start(bf16[2,16,128]{2,0,1:T(2,128)(2,1)} %bitcast.24), calls=%async_computation | async-start | bytes 16384 | tf_op jit(solution)/shard_map/all_to_all | solution.py:513
  9.0 0.0 copy-start.4
  9.0 0.0 copy-start.5
  9.0 0.0 copy-start.8
  9.0 0.0 copy-start.9
  9.0 0.0 copy-start.10
  9.0 0.0 copy-start.11
  9.1 0.0 copy-start.12
  9.1 0.0 copy-start.13
  9.1 0.0 copy-start.16
  9.1 0.0 copy-start.17
  9.1 0.0 copy-start.18
  9.1 0.0 copy-start.19
  9.2 0.0 copy-start.22
  9.2 0.1 collective-permute-start
  9.3 0.0 copy-start.23
  9.3 0.0 copy-start.24
  9.3 0.9 %copy-done.4 = bf16[2048,256]{1,0:T(8,128)(2,1)S(1)} copy-done((bf16[2048,256]{1,0:T(8,128)(2,1)S(1)}, bf16[2048,256]{1,0:T(8,128)(2,1)}, u32[]{:S(2)}) %copy-start.4) | copy-done | bytes 1048600
  10.2 0.3 copy-done.5
  10.6 2.2 %shard_map.274 = (f32[8,16,128]{2,1,0:T(8,128)S(1)}, f32[2,2,256]{2,1,0:T(2,128)S(1)}, f32[2,128]{1,0:T(2,128)S(1)}, bf16[2,3,2,256]{3,2,1,0:T(2,128)(2,1)}) custom-call(bf16[2,2048]{1,0:T(2,128)(2,1)S(1)} %copy-done.10, f32[1,2048]{1,0:T(1,128)S(1)} %bitcast.25, bf16[2048,256]{1,0:T(8,128)(2,1)S(1)} %copy-done.4, bf16[2048,256]{1,0:T(8,128)(2,1)S(1)} %copy-done.5, ...), custom_call_target="tpu_custom_call" | custom-call | tf_op jit(solution)/shard_map/pallas_call | solution.py:438
  12.8 3.4 %all-to-all-done = bf16[2,16,128]{2,0,1:T(2,128)(2,1)S(1)} async-done(((bf16[2,16,128]{2,0,1:T(2,128)(2,1)}), bf16[2,16,128]{2,0,1:T(2,128)(2,1)S(1)}, u32[]{:S(2)}, u32[]{:S(2)}) %all-to-all-start) | async-done | bytes 8224 | tf_op jit(solution)/shard_map/all_to_all | solution.py:513
  16.2 0.2 shard_map.275
  16.5 11.3 %all_to_all.39.terms_ref = bf16[16,40,128]{2,1,0:T(8,128)(2,1)S(1)} all-to-all(bf16[16,40,128]{2,1,0:T(8,128)(2,1)S(1)} %get-tuple-element.22), channel_id=1, replica_groups=mesh['ep'=16,'tp'=2] {'ep'}, dimensions={0} | all-to-all | bytes 327680 | tf_op jit(solution)/shard_map/all_to_all | solution.py:561
  27.7 0.1 shard_map.276
  27.9 9.2 %all_to_all.40.mix_ref = bf16[32,8,128]{2,1,0:T(8,128)(2,1)S(1)} all-to-all(bf16[32,8,128]{2,1,0:T(8,128)(2,1)S(1)} %get-tuple-element.24), channel_id=1, replica_groups=mesh['ep'=16,'tp'=2] {'ep','tp'}, dimensions={0} | all-to-all | bytes 131072 | tf_op jit(solution)/shard_map/all_to_all | solution.py:576
  37.1 0.0 copy-start.6
  37.1 0.0 copy-start.7
  37.2 0.2 shard_map.277
  37.4 10.2 %all_to_all.41.hid_ref = bf16[32,16,128]{2,1,0:T(8,128)(2,1)S(1)} all-to-all(bf16[32,16,128]{2,1,0:T(8,128)(2,1)S(1)} %shard_map.277), channel_id=1, replica_groups=mesh['ep'=16,'tp'=2] {'ep','tp'}, dimensions={0} | all-to-all | bytes 262144 | tf_op jit(solution)/shard_map/all_to_all | solution.py:586
  47.7 2.2 %shard_map.278 = (bf16[32,16,128]{2,1,0:T(8,128)(2,1)S(1)}, f32[16,128]{1,0:T(8,128)S(1)}, f32[2,16,64,128]{3,2,1,0:T(8,128)}, bf16[3,2,1024]{2,1,0:T(2,128)(2,1)}) custom-call(bf16[32,16,128]{2,1,0:T(8,128)(2,1)S(1)} %all_to_all.41.hid_ref, f32[32,128]{1,0:T(8,128)S(1)} %get-tuple-element.27.tail_ref, f32[16,128]{1,0:T(8,128)S(1)} %bitcast.28, ...), custom_call_target="tpu_custom_call" | custom-call | tf_op jit(solution)/shard_map/pallas_call | solution.py:438
  49.8 9.9 %all_to_all.42.terms_ref = bf16[32,16,128]{2,1,0:T(8,128)(2,1)S(1)} all-to-all(bf16[32,16,128]{2,1,0:T(8,128)(2,1)S(1)} %get-tuple-element.31), channel_id=1, replica_groups=mesh['ep'=16,'tp'=2] {'ep','tp'}, dimensions={0} | all-to-all | bytes 262144 | tf_op jit(solution)/shard_map/all_to_all | solution.py:625
  59.7 0.6 %final_stage.1 = bf16[1,2048]{1,0:T(2,128)(2,1)} custom-call(bf16[32,16,128]{2,1,0:T(8,128)(2,1)S(1)} %all_to_all.42.terms_ref, f32[16,128]{1,0:T(8,128)S(1)} %get-tuple-element.32.own_ref), custom_call_target="tpu_custom_call" | custom-call | tf_op jit(solution)/shard_map/final_stage/pallas_call | solution.py:464
  (35 shorter events, 0.1 us)
Async XLA Ops:
  0.6 15.6 %all-to-all-start = ((bf16[2,16,128]{2,0,1:T(2,128)(2,1)}), bf16[2,16,128]{2,0,1:T(2,128)(2,1)S(1)}, u32[]{:S(2)}, u32[]{:S(2)}) async-start(bf16[2,16,128]{2,0,1:T(2,128)(2,1)} %bitcast.24), calls=%async_computation | async-start | bytes 16384 | tf_op jit(solution)/shard_map/all_to_all | solution.py:513
  9.0 1.2 %copy-start.4 = (bf16[2048,256]{1,0:T(8,128)(2,1)S(1)}, bf16[2048,256]{1,0:T(8,128)(2,1)}, u32[]{:S(2)}) copy-start(bf16[2048,256]{1,0:T(8,128)(2,1)} %refs_2_.1) | copy-start | bytes 3145732
  9.0 1.5 %copy-start.5 = (bf16[2048,256]{1,0:T(8,128)(2,1)S(1)}, bf16[2048,256]{1,0:T(8,128)(2,1)}, u32[]{:S(2)}) copy-start(bf16[2048,256]{1,0:T(8,128)(2,1)} %refs_3_.1) | copy-start | bytes 3145732
  9.0 1.5 %copy-start.8 = (bf16[2048,16]{0,1:T(8,128)(2,1)S(1)}, bf16[2048,16]{0,1:T(8,128)(2,1)}, u32[]{:S(2)}) copy-start(bf16[2048,16]{0,1:T(8,128)(2,1)} %param.35) | copy-start | bytes 196612
  9.0 1.5 %copy-start.9 = (bf16[2,3,1024]{2,0,1:T(2,128)(2,1)S(1)}, bf16[2,3,1024]{2,0,1:T(2,128)(2,1)}, u32[]{:S(2)}) copy-start(bf16[2,3,1024]{2,0,1:T(2,128)(2,1)} %param.28) | copy-start | bytes 36868
  9.0 1.5 %copy-start.10 = (bf16[2,2048]{1,0:T(2,128)(2,1)S(1)}, bf16[2,2048]{1,0:T(2,128)(2,1)}, u32[]{:S(2)}) copy-start(bf16[2,2048]{1,0:T(2,128)(2,1)} %refs_0_.1) | copy-start | bytes 24580
  9.0 1.5 %copy-start.11 = (f32[4,1024]{1,0:T(4,128)S(1)}, f32[4,1024]{1,0:T(4,128)}, u32[]{:S(2)}) copy-start(f32[4,1024]{1,0:T(4,128)} %refs_7_.1) | copy-start | bytes 49156
  9.1 1.5 %copy-start.12 = (f32[4,2,256]{2,1,0:T(2,128)S(1)}, f32[4,2,256]{2,1,0:T(2,128)}, u32[]{:S(2)}) copy-start(f32[4,2,256]{2,1,0:T(2,128)} %refs_8_.1) | copy-start | bytes 24580
  9.1 1.5 %copy-start.13 = (f32[2048]{0:T(1024)S(1)}, f32[2048]{0:T(1024)}, u32[]{:S(2)}) copy-start(f32[2048]{0:T(1024)} %param.30) | copy-start | bytes 24580
  9.1 1.5 %copy-start.16 = (bf16[2,3,2,256]{3,2,1,0:T(2,128)(2,1)S(1)}, bf16[2,3,2,256]{3,2,1,0:T(2,128)(2,1)}, u32[]{:S(2)}) copy-start(bf16[2,3,2,256]{3,2,1,0:T(2,128)(2,1)} %refs_6_.1) | copy-start | bytes 18436
  9.1 1.5 %copy-start.17 = (f32[1024]{0:T(1024)S(1)}, f32[1024]{0:T(1024)}, u32[]{:S(2)}) copy-start(f32[1024]{0:T(1024)} %param.41) | copy-start | bytes 12292
  9.1 1.5 %copy-start.18 = (s32[2,4]{1,0:T(2,128)S(1)}, s32[2,4]{1,0:T(2,128)}, u32[]{:S(2)}) copy-start(s32[2,4]{1,0:T(2,128)} %refs_13_.1) | copy-start | bytes 100
  9.1 1.5 %copy-start.19 = (f32[16]{0:T(128)S(1)}, f32[16]{0:T(128)}, u32[]{:S(2)}) copy-start(f32[16]{0:T(128)} %param.38) | copy-start | bytes 196
  9.1 1.5 %copy-start.20 = (f32[16]{0:T(128)S(1)}, f32[16]{0:T(128)}, u32[]{:S(2)}) copy-start(f32[16]{0:T(128)} %param.39) | copy-start | bytes 196
  9.1 1.5 %copy-start.21 = (f32[16]{0:T(128)S(1)}, f32[16]{0:T(128)}, u32[]{:S(2)}) copy-start(f32[16]{0:T(128)} %param.40) | copy-start | bytes 196
  9.2 1.5 %copy-start.22 = (bf16[2,4]{1,0:T(2,128)(2,1)S(1)}, bf16[2,4]{1,0:T(2,128)(2,1)}, u32[]{:S(2)}) copy-start(bf16[2,4]{1,0:T(2,128)(2,1)} %refs_14_.1) | copy-start | bytes 52
  9.2 7.0 %collective-permute-start = (bf16[1024,128]{1,0:T(8,128)(2,1)}, bf16[1024,128]{1,0:T(8,128)(2,1)S(1)}, u32[]{:S(2)}, u32[]{:S(2)}) collective-permute-start(bf16[1024,128]{1,0:T(8,128)(2,1)} %own_ref.1), channel_id=1, source_target_pairs={{0,1},{1,0},{2,3},{3,2},{4,5},{5,4},{6,7},{7,6},{8,9},{9,8},{10,11... | collective-permute-start | bytes 786440 | tf_op jit(solution)/shard_map/ppermute | solution.py:516
  9.3 7.0 %copy-start.23 = (bf16[128,1024]{1,0:T(8,128)(2,1)S(1)}, bf16[128,1024]{1,0:T(8,128)(2,1)}, u32[]{:S(2)}) copy-start(bf16[128,1024]{1,0:T(8,128)(2,1)} %gate_ref.1) | copy-start | bytes 786436
  9.3 6.9 %copy-start.24 = (bf16[128,1024]{1,0:T(8,128)(2,1)S(1)}, bf16[128,1024]{1,0:T(8,128)(2,1)}, u32[]{:S(2)}) copy-start(bf16[128,1024]{1,0:T(8,128)(2,1)} %inner_ref.1) | copy-start | bytes 786436
  27.7 9.4 %copy-start.25 = (bf16[1024,128]{1,0:T(8,128)(2,1)S(1)}, bf16[1024,128]{1,0:T(8,128)(2,1)}, u32[]{:S(2)}) copy-start(bf16[1024,128]{1,0:T(8,128)(2,1)} %own_ref.1) | copy-start | bytes 786436
  37.1 10.5 %copy-start = (f32[2,16,64,128]{3,2,1,0:T(8,128)S(1)}, f32[2,16,64,128]{3,2,1,0:T(8,128)}, u32[]{:S(2)}) copy-start(f32[2,16,64,128]{3,2,1,0:T(8,128)} %state_ref.1) | copy-start | bytes 3145732
  37.1 10.5 %copy-start.1 = (bf16[1,2048,512]{2,1,0:T(8,128)(2,1)S(1)}, bf16[1,2048,512]{2,1,0:T(8,128)(2,1)}, u32[]{:S(2)}) copy-start(bf16[1,2048,512]{2,1,0:T(8,128)(2,1)} %param.46) | copy-start | bytes 6291460
  37.1 10.5 %copy-start.2 = (bf16[1,2048,512]{2,1,0:T(8,128)(2,1)S(1)}, bf16[1,2048,512]{2,1,0:T(8,128)(2,1)}, u32[]{:S(2)}) copy-start(bf16[1,2048,512]{2,1,0:T(8,128)(2,1)} %param.47) | copy-start | bytes 6291460
  37.1 10.5 %copy-start.3 = (bf16[1,512,2048]{2,1,0:T(8,128)(2,1)S(1)}, bf16[1,512,2048]{2,1,0:T(8,128)(2,1)}, u32[]{:S(2)}) copy-start(bf16[1,512,2048]{2,1,0:T(8,128)(2,1)} %param.48) | copy-start | bytes 6291460
  37.1 10.5 %copy-start.6 = (bf16[2048,128]{1,0:T(8,128)(2,1)S(1)}, bf16[2048,128]{1,0:T(8,128)(2,1)}, u32[]{:S(2)}) copy-start(bf16[2048,128]{1,0:T(8,128)(2,1)} %dup_ref.1) | copy-start | bytes 1572868
  37.1 10.5 %copy-start.7 = (bf16[128,2048]{1,0:T(8,128)(2,1)S(1)}, bf16[128,2048]{1,0:T(8,128)(2,1)}, u32[]{:S(2)}) copy-start(bf16[128,2048]{1,0:T(8,128)(2,1)} %ddown_ref.1) | copy-start | bytes 1572868
  37.2 10.5 %copy-start.14 = (f32[2048]{0:T(1024)S(1)}, f32[2048]{0:T(1024)}, u32[]{:S(2)}) copy-start(f32[2048]{0:T(1024)} %param.43) | copy-start | bytes 24580
  37.2 10.5 %copy-start.15 = (f32[2048]{0:T(1024)S(1)}, f32[2048]{0:T(1024)}, u32[]{:S(2)}) copy-start(f32[2048]{0:T(1024)} %param.51) | copy-start | bytes 24580
